TPU v7x, 512 devices: a whole 4x8x8 slice. The times are simulated.
512 devices in a mesh: fs: 64 (over z, y), tp: 8 (over x, core).
Axes of the slice: x: 4, y: 8, z: 8, core: 2. Of those that a mesh axis runs over, the one named last changes fastest.
Arguments:
- tokens: bfloat16 [24576, 2048], P('fs', 'tp'), may hold values from -60 to 60
- gain_mixer: float32 [2048], P('tp'), may hold values from 0.1 to 1.9
- w_in: bfloat16 [2048, 1024], P('fs', 'tp'), may hold values from -0.125 to 0.125
- pool_scale: float32 [1024], P('tp'), may hold values from 0.1 to 1.9
- w_pool_out: bfloat16 [2048, 1024], P('fs', 'tp'), may hold values from -0.5 to 0.5
- gain_mid: float32 [2048], P('tp'), may hold values from 0.1 to 1.9
- w_ff1: bfloat16 [2048, 8192], P('fs', 'tp'), may hold values from -0.125 to 0.125
- w_ff2: bfloat16 [2048, 8192], P('fs', 'tp'), may hold values from -0.1875 to 0.1875
- gain_out: float32 [2048], P('tp'), may hold values from 0.1 to 1.9
Outputs:
- layer_out: bfloat16 [24576, 2048], P('fs', 'tp')
All inputs are finite; a program needn't handle non-finite values.
Results may differ from a plain program's by a relative error of at most 0.017.
Values may be sent and summed in bfloat16 or wider, within the bound.
No kernel may reach another device: no remote copies, remote signals or barrier semaphores. Data moves between devices by JAX's collectives and lax.ppermute only.
A program may use at most 64 MiB of HBM per device.

v0:
```python
import functools

import jax
import jax.numpy as jnp
from jax import lax
from jax.experimental import pallas as pl
from jax.experimental.pallas import tpu as pltpu
from jax.sharding import Mesh, PartitionSpec as P


norm_eps = 1e-05
residual_alpha = 2.0**0.25
FS = ("z", "y")
TP = ("x", "core")
EVERY = FS + TP
bf16 = jnp.bfloat16
f32 = jnp.float32
OFFSETS = (0, -1, 1, -2, 2, -3, 3, -4)
MEBI = 1024 * 1024


def device(z, y, x, core):
    return (((z % 8) * 8 + y % 8) * 4 + x % 4) * 2 + core % 2


PLACES = [(z, y, x) for z in range(8) for y in range(8) for x in range(4)]
FIRST = [[device(z, y, x, 0) for z in range(8)] for y in range(8) for x in range(4)] + [
    [device(z, y, x, 1) for y in range(8)] for z in range(8) for x in range(4)
]
SECOND = [[device(z, y, x, 0) for y in range(8)] for z in range(8) for x in range(4)] + [
    [device(z, y, x, 1) for z in range(8)] for y in range(8) for x in range(4)
]


def around(steps):
    return [
        pair
        for z, y, x in PLACES
        for pair in (
            (device(z, y, x, 0), device(z, y + steps, x, 0)),
            (device(z, y, x, 1), device(z + steps, y, x, 1)),
        )
    ]


def along_x(array, steps):
    pairs = [
        (device(z, y, x, c), device(z, y, x + steps, c)) for z, y, x in PLACES for c in range(2)
    ]
    return lax.ppermute(array, EVERY, pairs)


def from_other_core(array):
    return lax.ppermute(array, "core", [(0, 1), (1, 0)])


def everyone(array, axis):
    count = lax.axis_size(axis)
    return lax.all_to_all(
        jnp.broadcast_to(array[None], (count, *array.shape)), axis, 0, 0, tiled=True
    )


def among(array, groups):
    return lax.all_to_all(
        jnp.broadcast_to(array[None], (8, *array.shape)),
        EVERY,
        0,
        0,
        axis_index_groups=groups,
        tiled=True,
    )


def scatter_sum_tp(keep, send):
    chip = (keep.astype(f32) + from_other_core(send).astype(f32)).astype(bf16)
    four = lax.all_to_all(chip, "x", 0, 0, tiled=True).astype(f32)
    return (four[0] + four[1]) + (four[2] + four[3])


def in_three(gain):
    rest, rows = gain, []
    for _ in range(3):
        rows.append(lax.reduce_precision(rest, 8, 7))
        rest = rest - rows[-1]
    return jnp.stack(rows).astype(bf16)


def gain_of(tok_ref, block, rows, first):
    parts = tok_ref[block, pl.ds(rows, 16), :].astype(f32)
    return parts[first : first + 1] + parts[first + 1 : first + 2] + parts[first + 2 : first + 3]


def columns_of(x, core):
    return pl.ds(pl.multiple_of((2 * x + core) * 256, 256), 256)


def row_at(core, source, j):
    at = jnp.where(core == 0, j * 256 + source * 32, source * 256 + j * 32)
    return pl.ds(pl.multiple_of(at, 32), 32)


def row_statistics(loads, width):
    total = None
    for load in loads:
        s = jnp.sum(load(), axis=1, keepdims=True)
        total = s if total is None else total + s
    mean = total / width
    spread = None
    for load in loads:
        c = load() - mean
        s = jnp.sum(c * c, axis=1, keepdims=True)
        spread = s if spread is None else spread + s
    return mean, lax.rsqrt(spread / width + norm_eps)


def shift_down(value, steps, row):
    return jnp.where(row >= steps, pltpu.roll(value, steps, 0), 0.0)


def mixed_kernel(rows, mine_ref, other_ref, mixed_ref):
    x, core = lax.axis_index("x"), lax.axis_index("core")
    step = rows // 3
    for t in range(3):
        part = pl.ds(t * step, step)
        blocks = [(ref, r) for ref in (mine_ref, other_ref) for r in range(4)]
        loads = [lambda ref=ref, r=r: ref[r, part, :].astype(f32) for ref, r in blocks]
        mean, inverse = row_statistics(loads, 2048)
        for (ref, r), load in zip(blocks, loads):
            where = columns_of(lax.rem(x + (4 - r), 4), core if ref is mine_ref else 1 - core)
            mixed = (load() - mean) * inverse * gain_of(ref, r, rows, 0)
            mixed_ref[part, where] = mixed.astype(bf16)


def mixer_kernel(mixed_ref, small_ref, scale_ref, keep_ref, send_ref, w_ref):
    x, core = lax.axis_index("x"), lax.axis_index("core")
    for s in range(8):
        for j in range(8):
            w_ref[row_at(core, s, j), :] = small_ref[s, j]
    pool_in = jnp.dot(mixed_ref[...], w_ref[:, :128], preferred_element_type=f32)
    u = pool_in.astype(bf16).astype(f32)
    row = lax.broadcasted_iota(jnp.int32, u.shape, 0)
    two = u + shift_down(u, 1, row)
    four = two + shift_down(two, 2, row)
    eight = four + shift_down(four, 4, row)
    sixteen = eight + shift_down(eight, 8, row)
    total = jnp.where(x == 0, two, jnp.where(x == 1, four, jnp.where(x == 2, eight, sixteen)))
    window = jnp.where(x == 0, 2, jnp.where(x == 1, 4, jnp.where(x == 2, 8, 16)))
    count = jnp.minimum(row + 1, window).astype(f32)
    pooled = ((total / count - u) * scale_ref[...]).astype(bf16)
    for xb in range(4):
        for ref, c in ((keep_ref, core), (send_ref, 1 - core)):
            term = lax.dot_general(
                pooled,
                w_ref[columns_of(xb, c), 128:],
                (((1,), (1,)), ((), ())),
                preferred_element_type=f32,
            )
            ref[xb] = term.astype(bf16)


def middle_kernel(rows, mine_ref, other_ref, mix_ref, mix_other_ref, mid_ref, own_ref):
    x, core = lax.axis_index("x"), lax.axis_index("core")
    step = rows // 3
    for t in range(3):
        part = pl.ds(t * step, step)
        blocks = [
            (tok, mix, c, xb)
            for tok, mix, c in ((mine_ref, mix_ref, core), (other_ref, mix_other_ref, 1 - core))
            for xb in range(4)
        ]

        def total(tok, mix, xb):
            r = lax.rem(x + (4 - xb), 4)
            return residual_alpha * tok[r, part, :].astype(f32) + mix[xb, part, :].astype(f32)

        loads = [functools.partial(total, tok, mix, xb) for tok, mix, _, xb in blocks]
        mean, inverse = row_statistics(loads, 2048)
        for (tok, mix, c, xb), load in zip(blocks, loads):
            gain = gain_of(tok, lax.rem(x + (4 - xb), 4), rows, 3)
            mid_ref[part, columns_of(xb, c)] = ((load() - mean) * inverse * gain).astype(bf16)
    own_ref[...] = mid_ref[:, columns_of(x, core)]


def ff_kernel(mid_ref, *refs):
    chunks, (keep_ref, send_ref, hid_ref, w_ref, sems) = refs[:8], refs[8:]
    core = lax.axis_index("core")
    place = jnp.where(core == 0, lax.axis_index("y"), lax.axis_index("z"))
    copies = [[], []]
    for half in range(2):
        where = pl.ds(half * 1024, 1024)
        for k, (chunk, offset) in enumerate(zip(chunks, OFFSETS)):
            source = lax.rem(place + (8 - offset), 8)
            for j in range(8):
                copy = pltpu.make_async_copy(
                    chunk.at[j, :, where],
                    w_ref.at[row_at(core, source, j), where],
                    sems.at[half, k, j],
                )
                copy.start()
                copies[half].append(copy)
    for copy in copies[0]:
        copy.wait()
    for n in range(4):
        where = slice(n * 256, (n + 1) * 256)
        up = jnp.dot(mid_ref[...], w_ref[:, where], preferred_element_type=f32)
        up = jnp.maximum(up, 0.0)
        hid_ref[:, where] = (up * up).astype(bf16)
    for copy in copies[1]:
        copy.wait()
    for xb in range(4):
        for ref, c in ((keep_ref, core), (send_ref, 1 - core)):
            term = lax.dot_general(
                hid_ref[...],
                w_ref[columns_of(xb, c), 1024:],
                (((1,), (1,)), ((), ())),
                preferred_element_type=f32,
            )
            ref[xb] = term.astype(bf16)


def vmem(count):
    return [pl.BlockSpec(memory_space=pltpu.VMEM)] * count


def mixed_of(mine, other, rows, width):
    return pl.pallas_call(
        functools.partial(mixed_kernel, rows),
        out_shape=jax.ShapeDtypeStruct((rows, 8 * width), bf16),
        in_specs=vmem(2),
        out_specs=vmem(1)[0],
        compiler_params=pltpu.CompilerParams(vmem_limit_bytes=16 * MEBI),
        cost_estimate=pl.CostEstimate(flops=2_000_000_000, bytes_accessed=3_000_000, transcendentals=0),
        name="mixed_in",
    )(mine, other)


def mixer(mixed, small, scale, rows, width, channels):
    block = jax.ShapeDtypeStruct((4, rows, width), bf16)
    return pl.pallas_call(
        mixer_kernel,
        out_shape=(block, block),
        in_specs=vmem(3),
        out_specs=tuple(vmem(2)),
        scratch_shapes=[pltpu.VMEM((8 * width, 2 * channels), bf16)],
        compiler_params=pltpu.CompilerParams(vmem_limit_bytes=24 * MEBI),
        cost_estimate=pl.CostEstimate(flops=2_000_000_000, bytes_accessed=4_000_000, transcendentals=0),
        name="mixer",
    )(mixed, small, scale)


def middle_of(mine, other, mix, mix_other, rows, width):
    return pl.pallas_call(
        functools.partial(middle_kernel, rows),
        out_shape=(
            jax.ShapeDtypeStruct((rows, 8 * width), bf16),
            jax.ShapeDtypeStruct((rows, width), bf16),
        ),
        in_specs=vmem(4),
        out_specs=tuple(vmem(2)),
        compiler_params=pltpu.CompilerParams(vmem_limit_bytes=16 * MEBI),
        cost_estimate=pl.CostEstimate(flops=2_000_000_000, bytes_accessed=5_000_000, transcendentals=0),
        name="middle",
    )(mine, other, mix, mix_other)


def feed_forward(full, chunks, rows, width):
    block = jax.ShapeDtypeStruct((4, rows, width), bf16)
    return pl.pallas_call(
        ff_kernel,
        out_shape=(block, block),
        in_specs=vmem(1) + [pl.BlockSpec(memory_space=pl.ANY)] * 8,
        out_specs=tuple(vmem(2)),
        scratch_shapes=[
            pltpu.VMEM((rows, 1024), bf16),
            pltpu.VMEM((2048, 2048), bf16),
            pltpu.SemaphoreType.DMA((2, 8, 8)),
        ],
        compiler_params=pltpu.CompilerParams(vmem_limit_bytes=30 * MEBI),
        cost_estimate=pl.CostEstimate(flops=6_000_000_000, bytes_accessed=12_000_000, transcendentals=0),
        name="feed_forward",
    )(full, *chunks)


def layer(tokens, gain_mixer, w_in, pool_scale, w_pool_out, gain_mid, w_ff1, w_ff2, gain_out):
    rows, width = tokens.shape
    channels = w_in.shape[1]
    packed = jnp.concatenate([w_ff1, w_ff2, w_in, w_pool_out], axis=1)
    first = among(packed, FIRST)
    small = among(first[:, :, 2048:].reshape(256, 2 * channels), SECOND)
    small = small.reshape(8, 8, 32, 2 * channels)
    chunk = first[:, :, :2048]
    chunks = [chunk]
    up, down = chunk, chunk
    for hop in range(4):
        down = lax.ppermute(down, EVERY, around(-1))
        chunks.append(down)
        if hop < 3:
            up = lax.ppermute(up, EVERY, around(1))
            chunks.append(up)
    extended = jnp.concatenate(
        [tokens, in_three(gain_mixer), in_three(gain_mid), jnp.zeros((10, width), bf16)]
    )
    pieces = [extended]
    for steps in (1, 2, 3):
        pieces.append(along_x(extended, steps))
    mine = jnp.stack(pieces)
    other = from_other_core(mine)
    mixed = mixed_of(mine, other, rows, width)
    keep, send = mixer(mixed, small, pool_scale[None], rows, width, channels)
    mixer_out = scatter_sum_tp(keep, send).astype(bf16)
    mix = everyone(mixer_out, "x")
    mix_other = from_other_core(mix)
    full, middle = middle_of(mine, other, mix, mix_other, rows, width)
    keep, send = feed_forward(full, chunks, rows, width)
    ff_out = scatter_sum_tp(keep, send).astype(bf16)
    value = residual_alpha * middle.astype(f32) + ff_out.astype(f32)
    part_mean = jnp.sum(value, axis=1) / width
    center = value - part_mean[:, None]
    part_spread = jnp.sum(center * center, axis=1)
    sums = jnp.concatenate([part_mean, part_spread])[None]
    means, spreads = jnp.split(everyone(sums, TP)[:, 0], 2, axis=1)
    mean = jnp.mean(means, axis=0)
    away = means - mean
    spread = (jnp.sum(spreads, axis=0) + width * jnp.sum(away * away, axis=0)) / (8 * width)
    result = (value - mean[:, None]) * lax.rsqrt(spread + norm_eps)[:, None] * gain_out
    return result.astype(bf16)


def solution(mesh):
    mesh = Mesh(mesh.devices.reshape(8, 8, 4, 2), EVERY)
    return jax.shard_map(
        layer,
        mesh=mesh,
        in_specs=(
            P(FS, TP),
            P(TP),
            P(FS, TP),
            P(TP),
            P(FS, TP),
            P(TP),
            P(FS, TP),
            P(FS, TP),
            P(TP),
        ),
        out_specs=P(FS, TP),
        check_vma=False,
    )
```

profile of v0, /device:TPU:1, one launch (start us, length us, event | category | flops | bytes accessed | tf_op | source)
XLA Modules:
  0.0 169.6 jit_solution(12250063547614682734)
XLA Ops:
  1.0 26.9 %all_to_all.30 = bf16[8,32,2304]{2,1,0:T(8,128)(2,1)S(1)} all-to-all(bf16[8,32,2304]{2,1,0:T(8,128)(2,1)S(1)} %broadcast_in_dim.17), channel_id=1, replica_groups={{0,64,128,192,256,320,384,448},{2,66,130,194,258,322,386,450},{4,68,132..., dimensions={0} | all-to-all | bytes 2359296 | tf_op jit(solution)/shard_map/all_to_all | solution.py:65
  30.0 9.7 %all-to-all-start.1 = ((bf16[8,256,256]{2,1,0:T(8,128)(2,1)}), bf16[8,256,256]{2,1,0:T(8,128)(2,1)S(1)}, u32[]{:S(2)}, u32[]{:S(2)}) async-start(bf16[8,256,256]{2,1,0:T(8,128)(2,1)} %broadcast_in_dim.19), calls=%async_computation.1 | async-start | bytes 2097152 | tf_op jit(solution)/shard_map/all_to_all | solution.py:65
  40.2 4.4 %collective-permute-start.2 = (bf16[400,256]{1,0:T(8,128)(2,1)S(1)}, bf16[400,256]{1,0:T(8,128)(2,1)S(1)}, u32[]{:S(2)}, u32[]{:S(2)}) collective-permute-start(bf16[400,256]{1,0:T(8,128)(2,1)S(1)} %concatenate.10), channel_id=1, source_target_pairs={{0,6},{1,7},{2,0},{3,1},{4,2},{5,3},{6,4},{7,5},{8,14},{9,15},{10,... | collective-permute-start | bytes 614408 | tf_op jit(solution)/shard_map/ppermute | solution.py:50
  44.6 2.4 %collective-permute-start.1 = (bf16[400,256]{1,0:T(8,128)(2,1)S(1)}, bf16[400,256]{1,0:T(8,128)(2,1)S(1)}, u32[]{:S(2)}, u32[]{:S(2)}) collective-permute-start(bf16[400,256]{1,0:T(8,128)(2,1)S(1)} %concatenate.10), channel_id=1, source_target_pairs={{0,4},{1,5},{2,6},{3,7},{4,0},{5,1},{6,2},{7,3},{8,12},{9,13},{10,... | collective-permute-start | bytes 614408 | tf_op jit(solution)/shard_map/ppermute | solution.py:50
  47.0 2.5 %collective-permute-start = (bf16[400,256]{1,0:T(8,128)(2,1)S(1)}, bf16[400,256]{1,0:T(8,128)(2,1)S(1)}, u32[]{:S(2)}, u32[]{:S(2)}) collective-permute-start(bf16[400,256]{1,0:T(8,128)(2,1)S(1)} %concatenate.10), channel_id=1, source_target_pairs={{0,2},{1,3},{2,4},{3,5},{4,6},{5,7},{6,0},{7,1},{8,10},{9,11},{10,... | collective-permute-start | bytes 614408 | tf_op jit(solution)/shard_map/ppermute | solution.py:50
  49.5 3.3 %collective-permute-done.1 = bf16[400,256]{1,0:T(8,128)(2,1)S(1)} collective-permute-done((bf16[400,256]{1,0:T(8,128)(2,1)S(1)}, bf16[400,256]{1,0:T(8,128)(2,1)S(1)}, u32[]{:S(2)}, u32[]{:S(2)}) %collective-permute-start.1) | collective-permute-done | bytes 204832 | tf_op jit(solution)/shard_map/ppermute | solution.py:50
  52.9 4.4 %collective-permute-done = bf16[400,256]{1,0:T(8,128)(2,1)S(1)} collective-permute-done((bf16[400,256]{1,0:T(8,128)(2,1)S(1)}, bf16[400,256]{1,0:T(8,128)(2,1)S(1)}, u32[]{:S(2)}, u32[]{:S(2)}) %collective-permute-start) | collective-permute-done | bytes 204832 | tf_op jit(solution)/shard_map/ppermute | solution.py:50
  57.4 4.4 %collective-permute-start.3 = (bf16[4,400,256]{2,1,0:T(8,128)(2,1)S(1)}, bf16[4,400,256]{2,1,0:T(8,128)(2,1)S(1)}, u32[]{:S(2)}, u32[]{:S(2)}) collective-permute-start(bf16[4,400,256]{2,1,0:T(8,128)(2,1)S(1)} %pad_maximum_fusion.mine_ref), channel_id=1, source_target_pairs={{0,1},{1,0},{2,3},{3,2},{4,5},{5,4},{6,7},{7,6},{8,9},{9,8},{10,11... | collective-permute-start | bytes 2457608 | tf_op jit(solution)/shard_map/ppermute | solution.py:54
  63.2 3.7 %collective-permute-start.6 = (bf16[8,32,2048]{2,1,0:T(8,128)(2,1)S(1)}, bf16[8,32,2048]{2,1,0:T(8,128)(2,1)}, u32[]{:S(2)}, u32[]{:S(2)}) collective-permute-start(bf16[8,32,2048]{2,1,0:T(8,128)(2,1)S(1)} %slice.45.refs_0_), channel_id=1, source_target_pairs={{0,56},{1,449},{2,58},{3,451},{4,60},{5,453},{6,62},{7,455},{8,0},... | collective-permute-start | bytes 3145736 | tf_op jit(solution)/shard_map/ppermute | solution.py:296
  72.1 1.9 %mixer.1 = (bf16[4,384,256]{2,1,0:T(8,128)(2,1)S(1)}, bf16[4,384,256]{2,1,0:T(8,128)(2,1)S(1)}) custom-call(bf16[384,2048]{1,0:T(8,128)(2,1)S(1)} %copy-done.4, bf16[8,8,32,256]{3,2,1,0:T(8,128)(2,1)S(1)} %bitcast.16, f32[1,128]{1,0:T(1,128)S(1)} %bitcast.17), custom_call_target="tpu_custom_call" | custom-call | flops 2000000000 | bytes 4000000 | tf_op jit(solution)/shard_map/mixer/pallas_call | solution.py:240
  74.1 2.3 %collective-permute-start.4 = (bf16[4,384,256]{2,1,0:T(8,128)(2,1)S(1)}, bf16[4,384,256]{2,1,0:T(8,128)(2,1)S(1)}, u32[]{:S(2)}, u32[]{:S(2)}) collective-permute-start(bf16[4,384,256]{2,1,0:T(8,128)(2,1)S(1)} %get-tuple-element.12), channel_id=1, source_target_pairs={{0,1},{1,0},{2,3},{3,2},{4,5},{5,4},{6,7},{7,6},{8,9},{9,8},{10,11... | collective-permute-start | bytes 2359304 | tf_op jit(solution)/shard_map/ppermute | solution.py:54
  76.4 2.2 %collective-permute-start.7 = (bf16[8,32,2048]{2,1,0:T(8,128)(2,1)S(1)}, bf16[8,32,2048]{2,1,0:T(8,128)(2,1)}, u32[]{:S(2)}, u32[]{:S(2)}) collective-permute-start(bf16[8,32,2048]{2,1,0:T(8,128)(2,1)S(1)} %slice.45.refs_0_), channel_id=1, source_target_pairs={{0,8},{1,65},{2,10},{3,67},{4,12},{5,69},{6,14},{7,71},{8,16},{9,7... | collective-permute-start | bytes 3145736 | tf_op jit(solution)/shard_map/ppermute | solution.py:299
  79.1 4.6 %collective-permute-start.8 = (bf16[8,32,2048]{2,1,0:T(8,128)(2,1)}, bf16[8,32,2048]{2,1,0:T(8,128)(2,1)}, u32[]{:S(2)}, u32[]{:S(2)}) collective-permute-start(bf16[8,32,2048]{2,1,0:T(8,128)(2,1)} %collective-permute-done.6.refs_1_), channel_id=1, source_target_pairs={{0,56},{1,449},{2,58},{3,451},{4,60},{5,453},{6,62},{7,455},{8,0},... | collective-permute-start | bytes 3145736 | tf_op jit(solution)/shard_map/ppermute | solution.py:296
  84.8 3.5 %all-to-all-start.2 = ((bf16[4,384,256]{2,1,0:T(8,128)(2,1)}), bf16[4,384,256]{2,1,0:T(8,128)(2,1)S(1)}, u32[]{:S(2)}, u32[]{:S(2)}) async-start(bf16[4,384,256]{2,1,0:T(8,128)(2,1)} %add_convert_fusion.1), calls=%async_computation.2 | async-start | bytes 1572864 | tf_op jit(solution)/shard_map/all_to_all | solution.py:77
  88.3 5.3 %collective-permute-done.7.refs_2_ = bf16[8,32,2048]{2,1,0:T(8,128)(2,1)} collective-permute-done((bf16[8,32,2048]{2,1,0:T(8,128)(2,1)S(1)}, bf16[8,32,2048]{2,1,0:T(8,128)(2,1)}, u32[]{:S(2)}, u32[]{:S(2)}) %collective-permute-start.7) | collective-permute-done | bytes 1048608 | tf_op jit(solution)/shard_map/ppermute | solution.py:299
  95.8 5.2 %collective-permute-start.10 = (bf16[8,32,2048]{2,1,0:T(8,128)(2,1)}, bf16[8,32,2048]{2,1,0:T(8,128)(2,1)}, u32[]{:S(2)}, u32[]{:S(2)}) collective-permute-start(bf16[8,32,2048]{2,1,0:T(8,128)(2,1)} %collective-permute-done.8.refs_3_), channel_id=1, source_target_pairs={{0,56},{1,449},{2,58},{3,451},{4,60},{5,453},{6,62},{7,455},{8,0},... | collective-permute-start | bytes 3145736 | tf_op jit(solution)/shard_map/ppermute | solution.py:296
  102.2 3.5 %all-to-all-start.3 = ((bf16[4,384,256]{2,1,0:T(8,128)(2,1)}), bf16[4,384,256]{2,1,0:T(8,128)(2,1)S(1)}, u32[]{:S(2)}, u32[]{:S(2)}) async-start(bf16[4,384,256]{2,1,0:T(8,128)(2,1)} %broadcast_in_dim.43), calls=%async_computation.3 | async-start | bytes 1572864 | tf_op jit(solution)/shard_map/all_to_all | solution.py:59
  105.7 5.2 %collective-permute-done.9.refs_4_ = bf16[8,32,2048]{2,1,0:T(8,128)(2,1)} collective-permute-done((bf16[8,32,2048]{2,1,0:T(8,128)(2,1)}, bf16[8,32,2048]{2,1,0:T(8,128)(2,1)}, u32[]{:S(2)}, u32[]{:S(2)}) %collective-permute-start.9) | collective-permute-done | bytes 1048608 | tf_op jit(solution)/shard_map/ppermute | solution.py:299
  113.0 5.2 %collective-permute-start.12 = (bf16[8,32,2048]{2,1,0:T(8,128)(2,1)}, bf16[8,32,2048]{2,1,0:T(8,128)(2,1)}, u32[]{:S(2)}, u32[]{:S(2)}) collective-permute-start(bf16[8,32,2048]{2,1,0:T(8,128)(2,1)} %collective-permute-done.10.refs_5_), channel_id=1, source_target_pairs={{0,56},{1,449},{2,58},{3,451},{4,60},{5,453},{6,62},{7,455},{8,0},... | collective-permute-start | bytes 3145736 | tf_op jit(solution)/shard_map/ppermute | solution.py:296
  118.2 5.4 %collective-permute-start.5 = (bf16[4,384,256]{2,1,0:T(8,128)(2,1)S(1)}, bf16[4,384,256]{2,1,0:T(8,128)(2,1)S(1)}, u32[]{:S(2)}, u32[]{:S(2)}) collective-permute-start(bf16[4,384,256]{2,1,0:T(8,128)(2,1)S(1)} %all-to-all-done.3.mix_ref), channel_id=1, source_target_pairs={{0,1},{1,0},{2,3},{3,2},{4,5},{5,4},{6,7},{7,6},{8,9},{9,8},{10,11... | collective-permute-start | bytes 2359304 | tf_op jit(solution)/shard_map/ppermute | solution.py:54
  130.2 7.1 %feed_forward.1 = (bf16[4,384,256]{2,1,0:T(8,128)(2,1)S(1)}, bf16[4,384,256]{2,1,0:T(8,128)(2,1)S(1)}) custom-call(bf16[384,2048]{1,0:T(8,128)(2,1)S(1)} %get-tuple-element.14.mid_ref, bf16[8,32,2048]{2,1,0:T(8,128)(2,1)S(1)} %slice.45.refs_0_, bf16[8,32,2048]{2,1,0:T(8,128)(2,1)} %collective-permute-done.6.refs_1_, ...), custom_call_target="tpu_custom_call" | custom-call | flops 6000000000 | bytes 12000000 | tf_op jit(solution)/shard_map/feed_forward/pallas_call | solution.py:269
  137.3 6.0 %collective-permute-start.13 = (bf16[4,384,256]{2,1,0:T(8,128)(2,1)S(1)}, bf16[4,384,256]{2,1,0:T(8,128)(2,1)S(1)}, u32[]{:S(2)}, u32[]{:S(2)}) collective-permute-start(bf16[4,384,256]{2,1,0:T(8,128)(2,1)S(1)} %get-tuple-element.16), channel_id=1, source_target_pairs={{0,1},{1,0},{2,3},{3,2},{4,5},{5,4},{6,7},{7,6},{8,9},{9,8},{10,11... | collective-permute-start | bytes 2359304 | tf_op jit(solution)/shard_map/ppermute | solution.py:54
  145.4 14.2 %all_to_all.31 = bf16[4,384,256]{2,1,0:T(8,128)(2,1)S(1)} all-to-all(bf16[4,384,256]{2,1,0:T(8,128)(2,1)S(1)} %add_convert_fusion), channel_id=1, replica_groups=mesh['z'=8,'y'=8,'x'=4,'core'=2] {'x'}, dimensions={0} | all-to-all | bytes 1572864 | tf_op jit(solution)/shard_map/all_to_all | solution.py:77
  160.3 8.5 %all_to_all.32 = f32[8,1,768]{2,1,0:T(1,128)S(1)} all-to-all(f32[8,1,768]{2,1,0:T(1,128)S(1)} %broadcast_in_dim.44), channel_id=1, replica_groups=mesh['z'=8,'y'=8,'x'=4,'core'=2] {'x','core'}, dimensions={0} | all-to-all | bytes 49152 | tf_op jit(solution)/shard_map/all_to_all | solution.py:59
  (70 shorter events, 27.2 us)
Async XLA Ops:
  29.0 10.8 %copy-start.8 = (f32[256]{0:T(256)S(1)}, f32[256]{0:T(256)}, u32[]{:S(2)}) copy-start(f32[256]{0:T(256)} %param.10) | copy-start | bytes 3076
  29.0 10.9 %copy-start.9 = (f32[256]{0:T(256)S(1)}, f32[256]{0:T(256)}, u32[]{:S(2)}) copy-start(f32[256]{0:T(256)} %param.14) | copy-start | bytes 3076
  29.0 10.9 %copy-start.6 = (bf16[384,256]{1,0:T(8,128)(2,1)S(1)}, bf16[384,256]{1,0:T(8,128)(2,1)}, u32[]{:S(2)}) copy-start(bf16[384,256]{1,0:T(8,128)(2,1)} %param.9) | copy-start | bytes 589828
  30.0 40.7 %all-to-all-start.1 = ((bf16[8,256,256]{2,1,0:T(8,128)(2,1)}), bf16[8,256,256]{2,1,0:T(8,128)(2,1)S(1)}, u32[]{:S(2)}, u32[]{:S(2)}) async-start(bf16[8,256,256]{2,1,0:T(8,128)(2,1)} %broadcast_in_dim.19), calls=%async_computation.1 | async-start | bytes 2097152 | tf_op jit(solution)/shard_map/all_to_all | solution.py:65
  40.2 9.4 %collective-permute-start.2 = (bf16[400,256]{1,0:T(8,128)(2,1)S(1)}, bf16[400,256]{1,0:T(8,128)(2,1)S(1)}, u32[]{:S(2)}, u32[]{:S(2)}) collective-permute-start(bf16[400,256]{1,0:T(8,128)(2,1)S(1)} %concatenate.10), channel_id=1, source_target_pairs={{0,6},{1,7},{2,0},{3,1},{4,2},{5,3},{6,4},{7,5},{8,14},{9,15},{10,... | collective-permute-start | bytes 614408 | tf_op jit(solution)/shard_map/ppermute | solution.py:50
  44.6 8.3 %collective-permute-start.1 = (bf16[400,256]{1,0:T(8,128)(2,1)S(1)}, bf16[400,256]{1,0:T(8,128)(2,1)S(1)}, u32[]{:S(2)}, u32[]{:S(2)}) collective-permute-start(bf16[400,256]{1,0:T(8,128)(2,1)S(1)} %concatenate.10), channel_id=1, source_target_pairs={{0,4},{1,5},{2,6},{3,7},{4,0},{5,1},{6,2},{7,3},{8,12},{9,13},{10,... | collective-permute-start | bytes 614408 | tf_op jit(solution)/shard_map/ppermute | solution.py:50
  47.0 10.3 %collective-permute-start = (bf16[400,256]{1,0:T(8,128)(2,1)S(1)}, bf16[400,256]{1,0:T(8,128)(2,1)S(1)}, u32[]{:S(2)}, u32[]{:S(2)}) collective-permute-start(bf16[400,256]{1,0:T(8,128)(2,1)S(1)} %concatenate.10), channel_id=1, source_target_pairs={{0,2},{1,3},{2,4},{3,5},{4,6},{5,7},{6,0},{7,1},{8,10},{9,11},{10,... | collective-permute-start | bytes 614408 | tf_op jit(solution)/shard_map/ppermute | solution.py:50
  57.4 9.5 %collective-permute-start.3 = (bf16[4,400,256]{2,1,0:T(8,128)(2,1)S(1)}, bf16[4,400,256]{2,1,0:T(8,128)(2,1)S(1)}, u32[]{:S(2)}, u32[]{:S(2)}) collective-permute-start(bf16[4,400,256]{2,1,0:T(8,128)(2,1)S(1)} %pad_maximum_fusion.mine_ref), channel_id=1, source_target_pairs={{0,1},{1,0},{2,3},{3,2},{4,5},{5,4},{6,7},{7,6},{8,9},{9,8},{10,11... | collective-permute-start | bytes 2457608 | tf_op jit(solution)/shard_map/ppermute | solution.py:54
  63.2 7.6 %copy-start.2 = (f32[128]{0:T(128)S(1)}, f32[128]{0:T(128)}, u32[]{:S(2)}) copy-start(f32[128]{0:T(128)} %param.12) | copy-start | bytes 1540
  63.2 15.9 %collective-permute-start.6 = (bf16[8,32,2048]{2,1,0:T(8,128)(2,1)S(1)}, bf16[8,32,2048]{2,1,0:T(8,128)(2,1)}, u32[]{:S(2)}, u32[]{:S(2)}) collective-permute-start(bf16[8,32,2048]{2,1,0:T(8,128)(2,1)S(1)} %slice.45.refs_0_), channel_id=1, source_target_pairs={{0,56},{1,449},{2,58},{3,451},{4,60},{5,453},{6,62},{7,455},{8,0},... | collective-permute-start | bytes 3145736 | tf_op jit(solution)/shard_map/ppermute | solution.py:296
  69.6 1.2 copy-start.3
  70.7 1.4 copy-start.4
  74.1 9.6 %collective-permute-start.4 = (bf16[4,384,256]{2,1,0:T(8,128)(2,1)S(1)}, bf16[4,384,256]{2,1,0:T(8,128)(2,1)S(1)}, u32[]{:S(2)}, u32[]{:S(2)}) collective-permute-start(bf16[4,384,256]{2,1,0:T(8,128)(2,1)S(1)} %get-tuple-element.12), channel_id=1, source_target_pairs={{0,1},{1,0},{2,3},{3,2},{4,5},{5,4},{6,7},{7,6},{8,9},{9,8},{10,11... | collective-permute-start | bytes 2359304 | tf_op jit(solution)/shard_map/ppermute | solution.py:54
  76.4 17.2 %collective-permute-start.7 = (bf16[8,32,2048]{2,1,0:T(8,128)(2,1)S(1)}, bf16[8,32,2048]{2,1,0:T(8,128)(2,1)}, u32[]{:S(2)}, u32[]{:S(2)}) collective-permute-start(bf16[8,32,2048]{2,1,0:T(8,128)(2,1)S(1)} %slice.45.refs_0_), channel_id=1, source_target_pairs={{0,8},{1,65},{2,10},{3,67},{4,12},{5,69},{6,14},{7,71},{8,16},{9,7... | collective-permute-start | bytes 3145736 | tf_op jit(solution)/shard_map/ppermute | solution.py:299
  79.1 16.6 %collective-permute-start.8 = (bf16[8,32,2048]{2,1,0:T(8,128)(2,1)}, bf16[8,32,2048]{2,1,0:T(8,128)(2,1)}, u32[]{:S(2)}, u32[]{:S(2)}) collective-permute-start(bf16[8,32,2048]{2,1,0:T(8,128)(2,1)} %collective-permute-done.6.refs_1_), channel_id=1, source_target_pairs={{0,56},{1,449},{2,58},{3,451},{4,60},{5,453},{6,62},{7,455},{8,0},... | collective-permute-start | bytes 3145736 | tf_op jit(solution)/shard_map/ppermute | solution.py:296
  84.8 16.2 %all-to-all-start.2 = ((bf16[4,384,256]{2,1,0:T(8,128)(2,1)}), bf16[4,384,256]{2,1,0:T(8,128)(2,1)S(1)}, u32[]{:S(2)}, u32[]{:S(2)}) async-start(bf16[4,384,256]{2,1,0:T(8,128)(2,1)} %add_convert_fusion.1), calls=%async_computation.2 | async-start | bytes 1572864 | tf_op jit(solution)/shard_map/all_to_all | solution.py:77
  93.6 17.4 %collective-permute-start.9 = (bf16[8,32,2048]{2,1,0:T(8,128)(2,1)}, bf16[8,32,2048]{2,1,0:T(8,128)(2,1)}, u32[]{:S(2)}, u32[]{:S(2)}) collective-permute-start(bf16[8,32,2048]{2,1,0:T(8,128)(2,1)} %collective-permute-done.7.refs_2_), channel_id=1, source_target_pairs={{0,8},{1,65},{2,10},{3,67},{4,12},{5,69},{6,14},{7,71},{8,16},{9,7... | collective-permute-start | bytes 3145736 | tf_op jit(solution)/shard_map/ppermute | solution.py:299
  95.8 17.2 %collective-permute-start.10 = (bf16[8,32,2048]{2,1,0:T(8,128)(2,1)}, bf16[8,32,2048]{2,1,0:T(8,128)(2,1)}, u32[]{:S(2)}, u32[]{:S(2)}) collective-permute-start(bf16[8,32,2048]{2,1,0:T(8,128)(2,1)} %collective-permute-done.8.refs_3_), channel_id=1, source_target_pairs={{0,56},{1,449},{2,58},{3,451},{4,60},{5,453},{6,62},{7,455},{8,0},... | collective-permute-start | bytes 3145736 | tf_op jit(solution)/shard_map/ppermute | solution.py:296
  102.2 16.0 %all-to-all-start.3 = ((bf16[4,384,256]{2,1,0:T(8,128)(2,1)}), bf16[4,384,256]{2,1,0:T(8,128)(2,1)S(1)}, u32[]{:S(2)}, u32[]{:S(2)}) async-start(bf16[4,384,256]{2,1,0:T(8,128)(2,1)} %broadcast_in_dim.43), calls=%async_computation.3 | async-start | bytes 1572864 | tf_op jit(solution)/shard_map/all_to_all | solution.py:59
  111.0 17.6 %collective-permute-start.11 = (bf16[8,32,2048]{2,1,0:T(8,128)(2,1)}, bf16[8,32,2048]{2,1,0:T(8,128)(2,1)}, u32[]{:S(2)}, u32[]{:S(2)}) collective-permute-start(bf16[8,32,2048]{2,1,0:T(8,128)(2,1)} %collective-permute-done.9.refs_4_), channel_id=1, source_target_pairs={{0,8},{1,65},{2,10},{3,67},{4,12},{5,69},{6,14},{7,71},{8,16},{9,7... | collective-permute-start | bytes 3145736 | tf_op jit(solution)/shard_map/ppermute | solution.py:299
  113.0 17.2 %collective-permute-start.12 = (bf16[8,32,2048]{2,1,0:T(8,128)(2,1)}, bf16[8,32,2048]{2,1,0:T(8,128)(2,1)}, u32[]{:S(2)}, u32[]{:S(2)}) collective-permute-start(bf16[8,32,2048]{2,1,0:T(8,128)(2,1)} %collective-permute-done.10.refs_5_), channel_id=1, source_target_pairs={{0,56},{1,449},{2,58},{3,451},{4,60},{5,453},{6,62},{7,455},{8,0},... | collective-permute-start | bytes 3145736 | tf_op jit(solution)/shard_map/ppermute | solution.py:296
  118.2 7.3 %collective-permute-start.5 = (bf16[4,384,256]{2,1,0:T(8,128)(2,1)S(1)}, bf16[4,384,256]{2,1,0:T(8,128)(2,1)S(1)}, u32[]{:S(2)}, u32[]{:S(2)}) collective-permute-start(bf16[4,384,256]{2,1,0:T(8,128)(2,1)S(1)} %all-to-all-done.3.mix_ref), channel_id=1, source_target_pairs={{0,1},{1,0},{2,3},{3,2},{4,5},{5,4},{6,7},{7,6},{8,9},{9,8},{10,11... | collective-permute-start | bytes 2359304 | tf_op jit(solution)/shard_map/ppermute | solution.py:54
  137.3 7.9 %collective-permute-start.13 = (bf16[4,384,256]{2,1,0:T(8,128)(2,1)S(1)}, bf16[4,384,256]{2,1,0:T(8,128)(2,1)S(1)}, u32[]{:S(2)}, u32[]{:S(2)}) collective-permute-start(bf16[4,384,256]{2,1,0:T(8,128)(2,1)S(1)} %get-tuple-element.16), channel_id=1, source_target_pairs={{0,1},{1,0},{2,3},{3,2},{4,5},{5,4},{6,7},{7,6},{8,9},{9,8},{10,11... | collective-permute-start | bytes 2359304 | tf_op jit(solution)/shard_map/ppermute | solution.py:54
  159.8 9.0 %copy-start.7 = (f32[256]{0:T(256)S(1)}, f32[256]{0:T(256)}, u32[]{:S(2)}) copy-start(f32[256]{0:T(256)} %param.17) | copy-start | bytes 3076
  (3 other events, 3.1 us)
where the time goes:
time: 171 us; the launch traced here: 170 us
  starting transfers between devices  68.9 us (40%)
  blocking collectives  49.6 us (29%)
  waiting for transfers between devices  24.7 us (14%)
  Pallas kernels  12.6 us (7%)
  local copies, waits for them, and re-layouts  9.42 us (6%)
  other arithmetic  3.99 us (2%)
    all_to_all x1, blocking collectives, among(): lax.all_to_all(jnp.broadcast_to(array[None], (8, *array.shape)), EVERY, 0...  26.9 us
    ppermute x4, starting transfers between devices, layer(): down = lax.ppermute(down, EVERY, around(-1))  18.7 us
    ppermute x4, starting transfers between devices, from_other_core(): return lax.ppermute(array, 'core', [(0, 1), (1, 0)])  18.2 us
    all_to_all x1, blocking collectives, scatter_sum_tp(): four = lax.all_to_all(chip, 'x', 0, 0, tiled=True).astype(f32)  14.2 us
    ppermute x3, waiting for transfers between devices, layer(): up = lax.ppermute(up, EVERY, around(1))  10.5 us
    all_to_all x1, starting transfers between devices, among(): lax.all_to_all(jnp.broadcast_to(array[None], (8, *array.shape)), EVERY, 0...  9.74 us
    ppermute x3, starting transfers between devices, along_x(): return lax.ppermute(array, EVERY, pairs)  9.33 us
    all_to_all x1, blocking collectives, everyone(): lax.all_to_all(jnp.broadcast_to(array[None], (count, *array.shape)), axis...  8.46 us
  transfers between devices with their start and end apart: 17, of which 10 were waited for; matrix products, arithmetic and copies ran while one was open for 2% of the time, Pallas kernels for 3%

commit v1 on v0

--- a/solution.py
+++ b/solution.py
@@ -118,8 +118,11 @@
     return jnp.where(row >= steps, pltpu.roll(value, steps, 0), 0.0)
 
 
-def mixed_kernel(rows, mine_ref, other_ref, mixed_ref):
+def mixer_kernel(rows, mine_ref, other_ref, small_ref, scale_ref, keep_ref, send_ref, mixed_ref, w_ref):
     x, core = lax.axis_index("x"), lax.axis_index("core")
+    for s in range(8):
+        for j in range(8):
+            w_ref[row_at(core, s, j), :] = small_ref[s, j]
     step = rows // 3
     for t in range(3):
         part = pl.ds(t * step, step)
@@ -130,13 +133,6 @@
             where = columns_of(lax.rem(x + (4 - r), 4), core if ref is mine_ref else 1 - core)
             mixed = (load() - mean) * inverse * gain_of(ref, r, rows, 0)
             mixed_ref[part, where] = mixed.astype(bf16)
-
-
-def mixer_kernel(mixed_ref, small_ref, scale_ref, keep_ref, send_ref, w_ref):
-    x, core = lax.axis_index("x"), lax.axis_index("core")
-    for s in range(8):
-        for j in range(8):
-            w_ref[row_at(core, s, j), :] = small_ref[s, j]
     pool_in = jnp.dot(mixed_ref[...], w_ref[:, :128], preferred_element_type=f32)
     u = pool_in.astype(bf16).astype(f32)
     row = lax.broadcasted_iota(jnp.int32, u.shape, 0)
@@ -223,30 +219,21 @@
     return [pl.BlockSpec(memory_space=pltpu.VMEM)] * count
 
 
-def mixed_of(mine, other, rows, width):
-    return pl.pallas_call(
-        functools.partial(mixed_kernel, rows),
-        out_shape=jax.ShapeDtypeStruct((rows, 8 * width), bf16),
-        in_specs=vmem(2),
-        out_specs=vmem(1)[0],
-        compiler_params=pltpu.CompilerParams(vmem_limit_bytes=16 * MEBI),
-        cost_estimate=pl.CostEstimate(flops=2_000_000_000, bytes_accessed=3_000_000, transcendentals=0),
-        name="mixed_in",
-    )(mine, other)
-
-
-def mixer(mixed, small, scale, rows, width, channels):
+def mixer(mine, other, small, scale, rows, width, channels):
     block = jax.ShapeDtypeStruct((4, rows, width), bf16)
     return pl.pallas_call(
-        mixer_kernel,
+        functools.partial(mixer_kernel, rows),
         out_shape=(block, block),
-        in_specs=vmem(3),
+        in_specs=vmem(4),
         out_specs=tuple(vmem(2)),
-        scratch_shapes=[pltpu.VMEM((8 * width, 2 * channels), bf16)],
+        scratch_shapes=[
+            pltpu.VMEM((rows, 8 * width), bf16),
+            pltpu.VMEM((8 * width, 2 * channels), bf16),
+        ],
         compiler_params=pltpu.CompilerParams(vmem_limit_bytes=24 * MEBI),
-        cost_estimate=pl.CostEstimate(flops=2_000_000_000, bytes_accessed=4_000_000, transcendentals=0),
+        cost_estimate=pl.CostEstimate(flops=4_000_000_000, bytes_accessed=4_000_000, transcendentals=0),
         name="mixer",
-    )(mixed, small, scale)
+    )(mine, other, small, scale)
 
 
 def middle_of(mine, other, mix, mix_other, rows, width):
@@ -306,8 +293,7 @@
         pieces.append(along_x(extended, steps))
     mine = jnp.stack(pieces)
     other = from_other_core(mine)
-    mixed = mixed_of(mine, other, rows, width)
-    keep, send = mixer(mixed, small, pool_scale[None], rows, width, channels)
+    keep, send = mixer(mine, other, small, pool_scale[None], rows, width, channels)
     mixer_out = scatter_sum_tp(keep, send).astype(bf16)
     mix = everyone(mixer_out, "x")
     mix_other = from_other_core(mix)

time: 171 us -> 171 us (level)
    ppermute x4, waiting for transfers between devices: 2.55 us -> 7.04 us  [layer(): down = lax.ppermute(down, EVERY, around(-1))]
    ppermute x3, waiting for transfers between devices: 10.5 us -> 7.57 us  [layer(): up = lax.ppermute(up, EVERY, around(1))]
    unnamed x21 -> x19, local copies, waits for them, and re-layouts: 5.69 us -> 4.29 us
    pallas_call x2 -> x1, Pallas kernels: 3.71 us -> 3.62 us  [mixer(): pl.pallas_call(functools.partial(mixer_kernel, rows), out_shape=(block, b...]
where the time goes in v1:
time: 171 us; the launch traced here: 170 us
  starting transfers between devices  68.9 us (40%)
  blocking collectives  49.6 us (29%)
  waiting for transfers between devices  26.2 us (15%)
  Pallas kernels  12.6 us (7%)
  local copies, waits for them, and re-layouts  7.97 us (5%)
  other arithmetic  3.98 us (2%)
    all_to_all x1, blocking collectives, among(): lax.all_to_all(jnp.broadcast_to(array[None], (8, *array.shape)), EVERY, 0...  26.9 us
    ppermute x4, starting transfers between devices, layer(): down = lax.ppermute(down, EVERY, around(-1))  18.7 us
    ppermute x4, starting transfers between devices, from_other_core(): return lax.ppermute(array, 'core', [(0, 1), (1, 0)])  18.2 us
    all_to_all x1, blocking collectives, scatter_sum_tp(): four = lax.all_to_all(chip, 'x', 0, 0, tiled=True).astype(f32)  14.2 us
    all_to_all x1, starting transfers between devices, among(): lax.all_to_all(jnp.broadcast_to(array[None], (8, *array.shape)), EVERY, 0...  9.74 us
    ppermute x3, starting transfers between devices, along_x(): return lax.ppermute(array, EVERY, pairs)  9.33 us
    all_to_all x1, blocking collectives, everyone(): lax.all_to_all(jnp.broadcast_to(array[None], (count, *array.shape)), axis...  8.45 us
    ppermute x3, waiting for transfers between devices, along_x(): return lax.ppermute(array, EVERY, pairs)  7.77 us
  transfers between devices with their start and end apart: 17, of which 10 were waited for; matrix products, arithmetic and copies ran while one was open for 2% of the time, Pallas kernels for 3%

profile of v1, /device:TPU:1, one launch (start us, length us, event | category | flops | bytes accessed | tf_op | source)
XLA Modules:
  0.0 169.6 jit_solution(9284189140015787935)
XLA Ops:
  1.0 26.9 %all_to_all.30 = bf16[8,32,2304]{2,1,0:T(8,128)(2,1)S(1)} all-to-all(bf16[8,32,2304]{2,1,0:T(8,128)(2,1)S(1)} %broadcast_in_dim.17), channel_id=1, replica_groups={{0,64,128,192,256,320,384,448},{2,66,130,194,258,322,386,450},{4,68,132..., dimensions={0} | all-to-all | bytes 2359296 | tf_op jit(solution)/shard_map/all_to_all | solution.py:65
  30.0 9.7 %all-to-all-start.1 = ((bf16[8,256,256]{2,1,0:T(8,128)(2,1)}), bf16[8,256,256]{2,1,0:T(8,128)(2,1)S(1)}, u32[]{:S(2)}, u32[]{:S(2)}) async-start(bf16[8,256,256]{2,1,0:T(8,128)(2,1)} %broadcast_in_dim.19), calls=%async_computation.1 | async-start | bytes 2097152 | tf_op jit(solution)/shard_map/all_to_all | solution.py:65
  40.1 4.4 %collective-permute-start.2 = (bf16[400,256]{1,0:T(8,128)(2,1)S(1)}, bf16[400,256]{1,0:T(8,128)(2,1)S(1)}, u32[]{:S(2)}, u32[]{:S(2)}) collective-permute-start(bf16[400,256]{1,0:T(8,128)(2,1)S(1)} %concatenate.10), channel_id=1, source_target_pairs={{0,6},{1,7},{2,0},{3,1},{4,2},{5,3},{6,4},{7,5},{8,14},{9,15},{10,... | collective-permute-start | bytes 614408 | tf_op jit(solution)/shard_map/ppermute | solution.py:50
  44.5 2.4 %collective-permute-start.1 = (bf16[400,256]{1,0:T(8,128)(2,1)S(1)}, bf16[400,256]{1,0:T(8,128)(2,1)S(1)}, u32[]{:S(2)}, u32[]{:S(2)}) collective-permute-start(bf16[400,256]{1,0:T(8,128)(2,1)S(1)} %concatenate.10), channel_id=1, source_target_pairs={{0,4},{1,5},{2,6},{3,7},{4,0},{5,1},{6,2},{7,3},{8,12},{9,13},{10,... | collective-permute-start | bytes 614408 | tf_op jit(solution)/shard_map/ppermute | solution.py:50
  47.0 2.5 %collective-permute-start = (bf16[400,256]{1,0:T(8,128)(2,1)S(1)}, bf16[400,256]{1,0:T(8,128)(2,1)S(1)}, u32[]{:S(2)}, u32[]{:S(2)}) collective-permute-start(bf16[400,256]{1,0:T(8,128)(2,1)S(1)} %concatenate.10), channel_id=1, source_target_pairs={{0,2},{1,3},{2,4},{3,5},{4,6},{5,7},{6,0},{7,1},{8,10},{9,11},{10,... | collective-permute-start | bytes 614408 | tf_op jit(solution)/shard_map/ppermute | solution.py:50
  49.5 3.3 %collective-permute-done.1 = bf16[400,256]{1,0:T(8,128)(2,1)S(1)} collective-permute-done((bf16[400,256]{1,0:T(8,128)(2,1)S(1)}, bf16[400,256]{1,0:T(8,128)(2,1)S(1)}, u32[]{:S(2)}, u32[]{:S(2)}) %collective-permute-start.1) | collective-permute-done | bytes 204832 | tf_op jit(solution)/shard_map/ppermute | solution.py:50
  52.8 4.4 %collective-permute-done = bf16[400,256]{1,0:T(8,128)(2,1)S(1)} collective-permute-done((bf16[400,256]{1,0:T(8,128)(2,1)S(1)}, bf16[400,256]{1,0:T(8,128)(2,1)S(1)}, u32[]{:S(2)}, u32[]{:S(2)}) %collective-permute-start) | collective-permute-done | bytes 204832 | tf_op jit(solution)/shard_map/ppermute | solution.py:50
  57.4 4.4 %collective-permute-start.3 = (bf16[4,400,256]{2,1,0:T(8,128)(2,1)S(1)}, bf16[4,400,256]{2,1,0:T(8,128)(2,1)S(1)}, u32[]{:S(2)}, u32[]{:S(2)}) collective-permute-start(bf16[4,400,256]{2,1,0:T(8,128)(2,1)S(1)} %pad_maximum_fusion.mine_ref), channel_id=1, source_target_pairs={{0,1},{1,0},{2,3},{3,2},{4,5},{5,4},{6,7},{7,6},{8,9},{9,8},{10,11... | collective-permute-start | bytes 2457608 | tf_op jit(solution)/shard_map/ppermute | solution.py:54
  63.1 3.7 %collective-permute-start.6 = (bf16[8,32,2048]{2,1,0:T(8,128)(2,1)S(1)}, bf16[8,32,2048]{2,1,0:T(8,128)(2,1)}, u32[]{:S(2)}, u32[]{:S(2)}) collective-permute-start(bf16[8,32,2048]{2,1,0:T(8,128)(2,1)S(1)} %slice.45.refs_0_), channel_id=1, source_target_pairs={{0,56},{1,449},{2,58},{3,451},{4,60},{5,453},{6,62},{7,455},{8,0},... | collective-permute-start | bytes 3145736 | tf_op jit(solution)/shard_map/ppermute | solution.py:283
  68.9 3.6 %mixer.1 = (bf16[4,384,256]{2,1,0:T(8,128)(2,1)S(1)}, bf16[4,384,256]{2,1,0:T(8,128)(2,1)S(1)}) custom-call(bf16[4,400,256]{2,1,0:T(8,128)(2,1)S(1)} %pad_maximum_fusion.mine_ref, bf16[4,400,256]{2,1,0:T(8,128)(2,1)S(1)} %copy-done.1, bf16[8,8,32,256]{3,2,1,0:T(8,128)(2,1)S(1)} %bitcast.16, f32[1,128]{1,0:T(1,128)S(1)} %bitcast.17), custom_call_target="tpu_custom_call" | custom-call | flops 4000000000 | bytes 4000000 | tf_op jit(solution)/shard_map/mixer/pallas_call | solution.py:224
  72.6 2.3 %collective-permute-start.4 = (bf16[4,384,256]{2,1,0:T(8,128)(2,1)S(1)}, bf16[4,384,256]{2,1,0:T(8,128)(2,1)S(1)}, u32[]{:S(2)}, u32[]{:S(2)}) collective-permute-start(bf16[4,384,256]{2,1,0:T(8,128)(2,1)S(1)} %get-tuple-element.12), channel_id=1, source_target_pairs={{0,1},{1,0},{2,3},{3,2},{4,5},{5,4},{6,7},{7,6},{8,9},{9,8},{10,11... | collective-permute-start | bytes 2359304 | tf_op jit(solution)/shard_map/ppermute | solution.py:54
  74.9 2.2 %collective-permute-start.7 = (bf16[8,32,2048]{2,1,0:T(8,128)(2,1)S(1)}, bf16[8,32,2048]{2,1,0:T(8,128)(2,1)}, u32[]{:S(2)}, u32[]{:S(2)}) collective-permute-start(bf16[8,32,2048]{2,1,0:T(8,128)(2,1)S(1)} %slice.45.refs_0_), channel_id=1, source_target_pairs={{0,8},{1,65},{2,10},{3,67},{4,12},{5,69},{6,14},{7,71},{8,16},{9,7... | collective-permute-start | bytes 3145736 | tf_op jit(solution)/shard_map/ppermute | solution.py:286
  79.1 4.6 %collective-permute-start.8 = (bf16[8,32,2048]{2,1,0:T(8,128)(2,1)}, bf16[8,32,2048]{2,1,0:T(8,128)(2,1)}, u32[]{:S(2)}, u32[]{:S(2)}) collective-permute-start(bf16[8,32,2048]{2,1,0:T(8,128)(2,1)} %collective-permute-done.6.refs_1_), channel_id=1, source_target_pairs={{0,56},{1,449},{2,58},{3,451},{4,60},{5,453},{6,62},{7,455},{8,0},... | collective-permute-start | bytes 3145736 | tf_op jit(solution)/shard_map/ppermute | solution.py:283
  84.8 3.5 %all-to-all-start.2 = ((bf16[4,384,256]{2,1,0:T(8,128)(2,1)}), bf16[4,384,256]{2,1,0:T(8,128)(2,1)S(1)}, u32[]{:S(2)}, u32[]{:S(2)}) async-start(bf16[4,384,256]{2,1,0:T(8,128)(2,1)} %add_convert_fusion.1), calls=%async_computation.2 | async-start | bytes 1572864 | tf_op jit(solution)/shard_map/all_to_all | solution.py:77
  88.3 3.8 %collective-permute-done.7.refs_2_ = bf16[8,32,2048]{2,1,0:T(8,128)(2,1)} collective-permute-done((bf16[8,32,2048]{2,1,0:T(8,128)(2,1)S(1)}, bf16[8,32,2048]{2,1,0:T(8,128)(2,1)}, u32[]{:S(2)}, u32[]{:S(2)}) %collective-permute-start.7) | collective-permute-done | bytes 1048608 | tf_op jit(solution)/shard_map/ppermute | solution.py:286
  95.7 5.2 %collective-permute-start.10 = (bf16[8,32,2048]{2,1,0:T(8,128)(2,1)}, bf16[8,32,2048]{2,1,0:T(8,128)(2,1)}, u32[]{:S(2)}, u32[]{:S(2)}) collective-permute-start(bf16[8,32,2048]{2,1,0:T(8,128)(2,1)} %collective-permute-done.8.refs_3_), channel_id=1, source_target_pairs={{0,56},{1,449},{2,58},{3,451},{4,60},{5,453},{6,62},{7,455},{8,0},... | collective-permute-start | bytes 3145736 | tf_op jit(solution)/shard_map/ppermute | solution.py:283
  102.2 3.5 %all-to-all-start.3 = ((bf16[4,384,256]{2,1,0:T(8,128)(2,1)}), bf16[4,384,256]{2,1,0:T(8,128)(2,1)S(1)}, u32[]{:S(2)}, u32[]{:S(2)}) async-start(bf16[4,384,256]{2,1,0:T(8,128)(2,1)} %broadcast_in_dim.43), calls=%async_computation.3 | async-start | bytes 1572864 | tf_op jit(solution)/shard_map/all_to_all | solution.py:59
  105.7 3.8 %collective-permute-done.9.refs_4_ = bf16[8,32,2048]{2,1,0:T(8,128)(2,1)} collective-permute-done((bf16[8,32,2048]{2,1,0:T(8,128)(2,1)}, bf16[8,32,2048]{2,1,0:T(8,128)(2,1)}, u32[]{:S(2)}, u32[]{:S(2)}) %collective-permute-start.9) | collective-permute-done | bytes 1048608 | tf_op jit(solution)/shard_map/ppermute | solution.py:286
  113.0 5.2 %collective-permute-start.12 = (bf16[8,32,2048]{2,1,0:T(8,128)(2,1)}, bf16[8,32,2048]{2,1,0:T(8,128)(2,1)}, u32[]{:S(2)}, u32[]{:S(2)}) collective-permute-start(bf16[8,32,2048]{2,1,0:T(8,128)(2,1)} %collective-permute-done.10.refs_5_), channel_id=1, source_target_pairs={{0,56},{1,449},{2,58},{3,451},{4,60},{5,453},{6,62},{7,455},{8,0},... | collective-permute-start | bytes 3145736 | tf_op jit(solution)/shard_map/ppermute | solution.py:283
  118.2 5.4 %collective-permute-start.5 = (bf16[4,384,256]{2,1,0:T(8,128)(2,1)S(1)}, bf16[4,384,256]{2,1,0:T(8,128)(2,1)S(1)}, u32[]{:S(2)}, u32[]{:S(2)}) collective-permute-start(bf16[4,384,256]{2,1,0:T(8,128)(2,1)S(1)} %all-to-all-done.3.mix_ref), channel_id=1, source_target_pairs={{0,1},{1,0},{2,3},{3,2},{4,5},{5,4},{6,7},{7,6},{8,9},{9,8},{10,11... | collective-permute-start | bytes 2359304 | tf_op jit(solution)/shard_map/ppermute | solution.py:54
  130.2 7.1 %feed_forward.1 = (bf16[4,384,256]{2,1,0:T(8,128)(2,1)S(1)}, bf16[4,384,256]{2,1,0:T(8,128)(2,1)S(1)}) custom-call(bf16[384,2048]{1,0:T(8,128)(2,1)S(1)} %get-tuple-element.14.mid_ref, bf16[8,32,2048]{2,1,0:T(8,128)(2,1)S(1)} %slice.45.refs_0_, bf16[8,32,2048]{2,1,0:T(8,128)(2,1)} %collective-permute-done.6.refs_1_, ...), custom_call_target="tpu_custom_call" | custom-call | flops 6000000000 | bytes 12000000 | tf_op jit(solution)/shard_map/feed_forward/pallas_call | solution.py:256
  137.3 6.0 %collective-permute-start.13 = (bf16[4,384,256]{2,1,0:T(8,128)(2,1)S(1)}, bf16[4,384,256]{2,1,0:T(8,128)(2,1)S(1)}, u32[]{:S(2)}, u32[]{:S(2)}) collective-permute-start(bf16[4,384,256]{2,1,0:T(8,128)(2,1)S(1)} %get-tuple-element.16), channel_id=1, source_target_pairs={{0,1},{1,0},{2,3},{3,2},{4,5},{5,4},{6,7},{7,6},{8,9},{9,8},{10,11... | collective-permute-start | bytes 2359304 | tf_op jit(solution)/shard_map/ppermute | solution.py:54
  145.4 14.2 %all_to_all.31 = bf16[4,384,256]{2,1,0:T(8,128)(2,1)S(1)} all-to-all(bf16[4,384,256]{2,1,0:T(8,128)(2,1)S(1)} %add_convert_fusion), channel_id=1, replica_groups=mesh['z'=8,'y'=8,'x'=4,'core'=2] {'x'}, dimensions={0} | all-to-all | bytes 1572864 | tf_op jit(solution)/shard_map/all_to_all | solution.py:77
  160.2 8.4 %all_to_all.32 = f32[8,1,768]{2,1,0:T(1,128)S(1)} all-to-all(f32[8,1,768]{2,1,0:T(1,128)S(1)} %broadcast_in_dim.44), channel_id=1, replica_groups=mesh['z'=8,'y'=8,'x'=4,'core'=2] {'x','core'}, dimensions={0} | all-to-all | bytes 49152 | tf_op jit(solution)/shard_map/all_to_all | solution.py:59
  (67 shorter events, 28.5 us)
Async XLA Ops:
  29.0 10.8 %copy-start.7 = (f32[256]{0:T(256)S(1)}, f32[256]{0:T(256)}, u32[]{:S(2)}) copy-start(f32[256]{0:T(256)} %param.10) | copy-start | bytes 3076
  29.0 10.8 %copy-start.8 = (f32[256]{0:T(256)S(1)}, f32[256]{0:T(256)}, u32[]{:S(2)}) copy-start(f32[256]{0:T(256)} %param.14) | copy-start | bytes 3076
  29.0 10.9 %copy-start.5 = (bf16[384,256]{1,0:T(8,128)(2,1)S(1)}, bf16[384,256]{1,0:T(8,128)(2,1)}, u32[]{:S(2)}) copy-start(bf16[384,256]{1,0:T(8,128)(2,1)} %param.9) | copy-start | bytes 589828
  30.0 37.8 %all-to-all-start.1 = ((bf16[8,256,256]{2,1,0:T(8,128)(2,1)}), bf16[8,256,256]{2,1,0:T(8,128)(2,1)S(1)}, u32[]{:S(2)}, u32[]{:S(2)}) async-start(bf16[8,256,256]{2,1,0:T(8,128)(2,1)} %broadcast_in_dim.19), calls=%async_computation.1 | async-start | bytes 2097152 | tf_op jit(solution)/shard_map/all_to_all | solution.py:65
  40.1 9.4 %collective-permute-start.2 = (bf16[400,256]{1,0:T(8,128)(2,1)S(1)}, bf16[400,256]{1,0:T(8,128)(2,1)S(1)}, u32[]{:S(2)}, u32[]{:S(2)}) collective-permute-start(bf16[400,256]{1,0:T(8,128)(2,1)S(1)} %concatenate.10), channel_id=1, source_target_pairs={{0,6},{1,7},{2,0},{3,1},{4,2},{5,3},{6,4},{7,5},{8,14},{9,15},{10,... | collective-permute-start | bytes 614408 | tf_op jit(solution)/shard_map/ppermute | solution.py:50
  44.5 8.3 %collective-permute-start.1 = (bf16[400,256]{1,0:T(8,128)(2,1)S(1)}, bf16[400,256]{1,0:T(8,128)(2,1)S(1)}, u32[]{:S(2)}, u32[]{:S(2)}) collective-permute-start(bf16[400,256]{1,0:T(8,128)(2,1)S(1)} %concatenate.10), channel_id=1, source_target_pairs={{0,4},{1,5},{2,6},{3,7},{4,0},{5,1},{6,2},{7,3},{8,12},{9,13},{10,... | collective-permute-start | bytes 614408 | tf_op jit(solution)/shard_map/ppermute | solution.py:50
  47.0 10.3 %collective-permute-start = (bf16[400,256]{1,0:T(8,128)(2,1)S(1)}, bf16[400,256]{1,0:T(8,128)(2,1)S(1)}, u32[]{:S(2)}, u32[]{:S(2)}) collective-permute-start(bf16[400,256]{1,0:T(8,128)(2,1)S(1)} %concatenate.10), channel_id=1, source_target_pairs={{0,2},{1,3},{2,4},{3,5},{4,6},{5,7},{6,0},{7,1},{8,10},{9,11},{10,... | collective-permute-start | bytes 614408 | tf_op jit(solution)/shard_map/ppermute | solution.py:50
  57.3 10.5 %copy-start.3 = (f32[128]{0:T(128)S(1)}, f32[128]{0:T(128)}, u32[]{:S(2)}) copy-start(f32[128]{0:T(128)} %param.12) | copy-start | bytes 1540
  57.4 9.4 %collective-permute-start.3 = (bf16[4,400,256]{2,1,0:T(8,128)(2,1)S(1)}, bf16[4,400,256]{2,1,0:T(8,128)(2,1)S(1)}, u32[]{:S(2)}, u32[]{:S(2)}) collective-permute-start(bf16[4,400,256]{2,1,0:T(8,128)(2,1)S(1)} %pad_maximum_fusion.mine_ref), channel_id=1, source_target_pairs={{0,1},{1,0},{2,3},{3,2},{4,5},{5,4},{6,7},{7,6},{8,9},{9,8},{10,11... | collective-permute-start | bytes 2457608 | tf_op jit(solution)/shard_map/ppermute | solution.py:54
  63.1 15.9 %collective-permute-start.6 = (bf16[8,32,2048]{2,1,0:T(8,128)(2,1)S(1)}, bf16[8,32,2048]{2,1,0:T(8,128)(2,1)}, u32[]{:S(2)}, u32[]{:S(2)}) collective-permute-start(bf16[8,32,2048]{2,1,0:T(8,128)(2,1)S(1)} %slice.45.refs_0_), channel_id=1, source_target_pairs={{0,56},{1,449},{2,58},{3,451},{4,60},{5,453},{6,62},{7,455},{8,0},... | collective-permute-start | bytes 3145736 | tf_op jit(solution)/shard_map/ppermute | solution.py:283
  67.8 1.1 copy-start.1
  72.6 11.1 %collective-permute-start.4 = (bf16[4,384,256]{2,1,0:T(8,128)(2,1)S(1)}, bf16[4,384,256]{2,1,0:T(8,128)(2,1)S(1)}, u32[]{:S(2)}, u32[]{:S(2)}) collective-permute-start(bf16[4,384,256]{2,1,0:T(8,128)(2,1)S(1)} %get-tuple-element.12), channel_id=1, source_target_pairs={{0,1},{1,0},{2,3},{3,2},{4,5},{5,4},{6,7},{7,6},{8,9},{9,8},{10,11... | collective-permute-start | bytes 2359304 | tf_op jit(solution)/shard_map/ppermute | solution.py:54
  74.9 17.2 %collective-permute-start.7 = (bf16[8,32,2048]{2,1,0:T(8,128)(2,1)S(1)}, bf16[8,32,2048]{2,1,0:T(8,128)(2,1)}, u32[]{:S(2)}, u32[]{:S(2)}) collective-permute-start(bf16[8,32,2048]{2,1,0:T(8,128)(2,1)S(1)} %slice.45.refs_0_), channel_id=1, source_target_pairs={{0,8},{1,65},{2,10},{3,67},{4,12},{5,69},{6,14},{7,71},{8,16},{9,7... | collective-permute-start | bytes 3145736 | tf_op jit(solution)/shard_map/ppermute | solution.py:286
  79.1 16.6 %collective-permute-start.8 = (bf16[8,32,2048]{2,1,0:T(8,128)(2,1)}, bf16[8,32,2048]{2,1,0:T(8,128)(2,1)}, u32[]{:S(2)}, u32[]{:S(2)}) collective-permute-start(bf16[8,32,2048]{2,1,0:T(8,128)(2,1)} %collective-permute-done.6.refs_1_), channel_id=1, source_target_pairs={{0,56},{1,449},{2,58},{3,451},{4,60},{5,453},{6,62},{7,455},{8,0},... | collective-permute-start | bytes 3145736 | tf_op jit(solution)/shard_map/ppermute | solution.py:283
  84.8 16.2 %all-to-all-start.2 = ((bf16[4,384,256]{2,1,0:T(8,128)(2,1)}), bf16[4,384,256]{2,1,0:T(8,128)(2,1)S(1)}, u32[]{:S(2)}, u32[]{:S(2)}) async-start(bf16[4,384,256]{2,1,0:T(8,128)(2,1)} %add_convert_fusion.1), calls=%async_computation.2 | async-start | bytes 1572864 | tf_op jit(solution)/shard_map/all_to_all | solution.py:77
  92.1 17.4 %collective-permute-start.9 = (bf16[8,32,2048]{2,1,0:T(8,128)(2,1)}, bf16[8,32,2048]{2,1,0:T(8,128)(2,1)}, u32[]{:S(2)}, u32[]{:S(2)}) collective-permute-start(bf16[8,32,2048]{2,1,0:T(8,128)(2,1)} %collective-permute-done.7.refs_2_), channel_id=1, source_target_pairs={{0,8},{1,65},{2,10},{3,67},{4,12},{5,69},{6,14},{7,71},{8,16},{9,7... | collective-permute-start | bytes 3145736 | tf_op jit(solution)/shard_map/ppermute | solution.py:286
  95.7 17.2 %collective-permute-start.10 = (bf16[8,32,2048]{2,1,0:T(8,128)(2,1)}, bf16[8,32,2048]{2,1,0:T(8,128)(2,1)}, u32[]{:S(2)}, u32[]{:S(2)}) collective-permute-start(bf16[8,32,2048]{2,1,0:T(8,128)(2,1)} %collective-permute-done.8.refs_3_), channel_id=1, source_target_pairs={{0,56},{1,449},{2,58},{3,451},{4,60},{5,453},{6,62},{7,455},{8,0},... | collective-permute-start | bytes 3145736 | tf_op jit(solution)/shard_map/ppermute | solution.py:283
  102.2 16.0 %all-to-all-start.3 = ((bf16[4,384,256]{2,1,0:T(8,128)(2,1)}), bf16[4,384,256]{2,1,0:T(8,128)(2,1)S(1)}, u32[]{:S(2)}, u32[]{:S(2)}) async-start(bf16[4,384,256]{2,1,0:T(8,128)(2,1)} %broadcast_in_dim.43), calls=%async_computation.3 | async-start | bytes 1572864 | tf_op jit(solution)/shard_map/all_to_all | solution.py:59
  109.4 19.1 %collective-permute-start.11 = (bf16[8,32,2048]{2,1,0:T(8,128)(2,1)}, bf16[8,32,2048]{2,1,0:T(8,128)(2,1)}, u32[]{:S(2)}, u32[]{:S(2)}) collective-permute-start(bf16[8,32,2048]{2,1,0:T(8,128)(2,1)} %collective-permute-done.9.refs_4_), channel_id=1, source_target_pairs={{0,8},{1,65},{2,10},{3,67},{4,12},{5,69},{6,14},{7,71},{8,16},{9,7... | collective-permute-start | bytes 3145736 | tf_op jit(solution)/shard_map/ppermute | solution.py:286
  113.0 17.2 %collective-permute-start.12 = (bf16[8,32,2048]{2,1,0:T(8,128)(2,1)}, bf16[8,32,2048]{2,1,0:T(8,128)(2,1)}, u32[]{:S(2)}, u32[]{:S(2)}) collective-permute-start(bf16[8,32,2048]{2,1,0:T(8,128)(2,1)} %collective-permute-done.10.refs_5_), channel_id=1, source_target_pairs={{0,56},{1,449},{2,58},{3,451},{4,60},{5,453},{6,62},{7,455},{8,0},... | collective-permute-start | bytes 3145736 | tf_op jit(solution)/shard_map/ppermute | solution.py:283
  118.2 7.3 %collective-permute-start.5 = (bf16[4,384,256]{2,1,0:T(8,128)(2,1)S(1)}, bf16[4,384,256]{2,1,0:T(8,128)(2,1)S(1)}, u32[]{:S(2)}, u32[]{:S(2)}) collective-permute-start(bf16[4,384,256]{2,1,0:T(8,128)(2,1)S(1)} %all-to-all-done.3.mix_ref), channel_id=1, source_target_pairs={{0,1},{1,0},{2,3},{3,2},{4,5},{5,4},{6,7},{7,6},{8,9},{9,8},{10,11... | collective-permute-start | bytes 2359304 | tf_op jit(solution)/shard_map/ppermute | solution.py:54
  125.5 1.1 copy-start.2
  137.3 7.9 %collective-permute-start.13 = (bf16[4,384,256]{2,1,0:T(8,128)(2,1)S(1)}, bf16[4,384,256]{2,1,0:T(8,128)(2,1)S(1)}, u32[]{:S(2)}, u32[]{:S(2)}) collective-permute-start(bf16[4,384,256]{2,1,0:T(8,128)(2,1)S(1)} %get-tuple-element.16), channel_id=1, source_target_pairs={{0,1},{1,0},{2,3},{3,2},{4,5},{5,4},{6,7},{7,6},{8,9},{9,8},{10,11... | collective-permute-start | bytes 2359304 | tf_op jit(solution)/shard_map/ppermute | solution.py:54
  159.8 9.0 %copy-start.6 = (f32[256]{0:T(256)S(1)}, f32[256]{0:T(256)}, u32[]{:S(2)}) copy-start(f32[256]{0:T(256)} %param.17) | copy-start | bytes 3076
  (2 other events, 2.0 us)

commit v2 on v1

--- a/solution.py
+++ b/solution.py
@@ -61,15 +61,12 @@
     )
 
 
-def among(array, groups):
-    return lax.all_to_all(
-        jnp.broadcast_to(array[None], (8, *array.shape)),
-        EVERY,
-        0,
-        0,
-        axis_index_groups=groups,
-        tiled=True,
-    )
+def eight(array):
+    return jnp.broadcast_to(array[None], (8, *array.shape))
+
+
+def exchanged(blocks, groups):
+    return lax.all_to_all(blocks, EVERY, 0, 0, axis_index_groups=groups, tiled=True)
 
 
 def scatter_sum_tp(keep, send):
@@ -219,6 +216,34 @@
     return [pl.BlockSpec(memory_space=pltpu.VMEM)] * count
 
 
+def split_kernel(first_ref, chunk_ref, blocks_ref, small_ref, sems):
+    small = pltpu.make_async_copy(first_ref.at[:, :, pl.ds(2048, 256)], small_ref, sems.at[0])
+    chunk = pltpu.make_async_copy(first_ref.at[:, :, pl.ds(0, 2048)], chunk_ref, sems.at[1])
+    small.start()
+    chunk.start()
+    small.wait()
+    rows = small_ref[...].reshape(256, 256)
+    for i in range(8):
+        blocks_ref[i] = rows
+    chunk.wait()
+
+
+def split(first):
+    return pl.pallas_call(
+        split_kernel,
+        out_shape=(
+            jax.ShapeDtypeStruct((8, 32, 2048), bf16),
+            jax.ShapeDtypeStruct((8, 256, 256), bf16),
+        ),
+        in_specs=[pl.BlockSpec(memory_space=pl.ANY)],
+        out_specs=tuple(vmem(2)),
+        scratch_shapes=[pltpu.VMEM((8, 32, 256), bf16), pltpu.SemaphoreType.DMA((2,))],
+        compiler_params=pltpu.CompilerParams(vmem_limit_bytes=8 * MEBI),
+        cost_estimate=pl.CostEstimate(flops=1_000_000, bytes_accessed=3_000_000, transcendentals=0),
+        name="split",
+    )(first)
+
+
 def mixer(mine, other, small, scale, rows, width, channels):
     block = jax.ShapeDtypeStruct((4, rows, width), bf16)
     return pl.pallas_call(
@@ -273,10 +298,10 @@
     rows, width = tokens.shape
     channels = w_in.shape[1]
     packed = jnp.concatenate([w_ff1, w_ff2, w_in, w_pool_out], axis=1)
-    first = among(packed, FIRST)
-    small = among(first[:, :, 2048:].reshape(256, 2 * channels), SECOND)
+    first = exchanged(eight(packed), FIRST)
+    chunk, blocks = split(first)
+    small = exchanged(blocks, SECOND)
     small = small.reshape(8, 8, 32, 2 * channels)
-    chunk = first[:, :, :2048]
     chunks = [chunk]
     up, down = chunk, chunk
     for hop in range(4):

time: 171 us -> 168 us (0.982)
  local copies, waits for them, and re-layouts: 7.97 us -> 4.6 us
    unnamed x19 -> x17, local copies, waits for them, and re-layouts: 4.29 us -> 3.24 us
where the time goes in v2:
time: 168 us; the launch traced here: 167 us
  starting transfers between devices  68.9 us (41%)
  blocking collectives  49.6 us (30%)
  waiting for transfers between devices  26.2 us (16%)
  Pallas kernels  13.7 us (8%)
  local copies, waits for them, and re-layouts  4.6 us (3%)
  other arithmetic  3.98 us (2%)
    all_to_all x1, blocking collectives, exchanged(): lax.all_to_all(blocks, EVERY, 0, 0, axis_index_groups=groups, tiled=True)  26.9 us
    ppermute x4, starting transfers between devices, layer(): down = lax.ppermute(down, EVERY, around(-1))  18.7 us
    ppermute x4, starting transfers between devices, from_other_core(): return lax.ppermute(array, 'core', [(0, 1), (1, 0)])  18.1 us
    all_to_all x1, blocking collectives, scatter_sum_tp(): four = lax.all_to_all(chip, 'x', 0, 0, tiled=True).astype(f32)  14.2 us
    all_to_all x1, starting transfers between devices, exchanged(): lax.all_to_all(blocks, EVERY, 0, 0, axis_index_groups=groups, tiled=True)  9.75 us
    ppermute x3, starting transfers between devices, along_x(): return lax.ppermute(array, EVERY, pairs)  9.33 us
    all_to_all x1, blocking collectives, everyone(): lax.all_to_all(jnp.broadcast_to(array[None], (count, *array.shape)), axis...  8.45 us
    ppermute x3, waiting for transfers between devices, along_x(): return lax.ppermute(array, EVERY, pairs)  7.77 us
  transfers between devices with their start and end apart: 17, of which 10 were waited for; matrix products, arithmetic and copies ran while one was open for 2% of the time, Pallas kernels for 3%

profile of v2, /device:TPU:1, one launch (start us, length us, event | category | flops | bytes accessed | tf_op | source)
XLA Modules:
  0.0 167.4 jit_solution(4437216103981343302)
XLA Ops:
  1.0 26.9 %all_to_all.30.first_ref = bf16[8,32,2304]{2,1,0:T(8,128)(2,1)S(1)} all-to-all(bf16[8,32,2304]{2,1,0:T(8,128)(2,1)S(1)} %broadcast_in_dim.13), channel_id=1, replica_groups={{0,64,128,192,256,320,384,448},{2,66,130,194,258,322,386,450},{4,68,132..., dimensions={0} | all-to-all | bytes 2359296 | tf_op jit(solution)/shard_map/all_to_all | solution.py:69
  29.1 9.8 %all-to-all-start.1 = ((bf16[8,256,256]{2,1,0:T(8,128)(2,1)}), bf16[8,256,256]{2,1,0:T(8,128)(2,1)S(1)}, u32[]{:S(2)}, u32[]{:S(2)}) async-start(bf16[8,256,256]{2,1,0:T(8,128)(2,1)} %get-tuple-element.13), calls=%async_computation.1 | async-start | bytes 2097152 | tf_op jit(solution)/shard_map/all_to_all | solution.py:69
  39.2 4.4 %collective-permute-start.2 = (bf16[400,256]{1,0:T(8,128)(2,1)S(1)}, bf16[400,256]{1,0:T(8,128)(2,1)S(1)}, u32[]{:S(2)}, u32[]{:S(2)}) collective-permute-start(bf16[400,256]{1,0:T(8,128)(2,1)S(1)} %concatenate.10), channel_id=1, source_target_pairs={{0,6},{1,7},{2,0},{3,1},{4,2},{5,3},{6,4},{7,5},{8,14},{9,15},{10,... | collective-permute-start | bytes 614408 | tf_op jit(solution)/shard_map/ppermute | solution.py:50
  43.6 2.4 %collective-permute-start.1 = (bf16[400,256]{1,0:T(8,128)(2,1)S(1)}, bf16[400,256]{1,0:T(8,128)(2,1)S(1)}, u32[]{:S(2)}, u32[]{:S(2)}) collective-permute-start(bf16[400,256]{1,0:T(8,128)(2,1)S(1)} %concatenate.10), channel_id=1, source_target_pairs={{0,4},{1,5},{2,6},{3,7},{4,0},{5,1},{6,2},{7,3},{8,12},{9,13},{10,... | collective-permute-start | bytes 614408 | tf_op jit(solution)/shard_map/ppermute | solution.py:50
  46.0 2.5 %collective-permute-start = (bf16[400,256]{1,0:T(8,128)(2,1)S(1)}, bf16[400,256]{1,0:T(8,128)(2,1)S(1)}, u32[]{:S(2)}, u32[]{:S(2)}) collective-permute-start(bf16[400,256]{1,0:T(8,128)(2,1)S(1)} %concatenate.10), channel_id=1, source_target_pairs={{0,2},{1,3},{2,4},{3,5},{4,6},{5,7},{6,0},{7,1},{8,10},{9,11},{10,... | collective-permute-start | bytes 614408 | tf_op jit(solution)/shard_map/ppermute | solution.py:50
  48.6 3.3 %collective-permute-done.1 = bf16[400,256]{1,0:T(8,128)(2,1)S(1)} collective-permute-done((bf16[400,256]{1,0:T(8,128)(2,1)S(1)}, bf16[400,256]{1,0:T(8,128)(2,1)S(1)}, u32[]{:S(2)}, u32[]{:S(2)}) %collective-permute-start.1) | collective-permute-done | bytes 204832 | tf_op jit(solution)/shard_map/ppermute | solution.py:50
  51.9 4.4 %collective-permute-done = bf16[400,256]{1,0:T(8,128)(2,1)S(1)} collective-permute-done((bf16[400,256]{1,0:T(8,128)(2,1)S(1)}, bf16[400,256]{1,0:T(8,128)(2,1)S(1)}, u32[]{:S(2)}, u32[]{:S(2)}) %collective-permute-start) | collective-permute-done | bytes 204832 | tf_op jit(solution)/shard_map/ppermute | solution.py:50
  56.5 4.4 %collective-permute-start.3 = (bf16[4,400,256]{2,1,0:T(8,128)(2,1)S(1)}, bf16[4,400,256]{2,1,0:T(8,128)(2,1)S(1)}, u32[]{:S(2)}, u32[]{:S(2)}) collective-permute-start(bf16[4,400,256]{2,1,0:T(8,128)(2,1)S(1)} %pad_maximum_fusion.mine_ref), channel_id=1, source_target_pairs={{0,1},{1,0},{2,3},{3,2},{4,5},{5,4},{6,7},{7,6},{8,9},{9,8},{10,11... | collective-permute-start | bytes 2457608 | tf_op jit(solution)/shard_map/ppermute | solution.py:54
  60.9 3.7 %collective-permute-start.6 = (bf16[8,32,2048]{2,1,0:T(8,128)(2,1)S(1)}, bf16[8,32,2048]{2,1,0:T(8,128)(2,1)}, u32[]{:S(2)}, u32[]{:S(2)}) collective-permute-start(bf16[8,32,2048]{2,1,0:T(8,128)(2,1)S(1)} %get-tuple-element.18.refs_0_), channel_id=1, source_target_pairs={{0,56},{1,449},{2,58},{3,451},{4,60},{5,453},{6,62},{7,455},{8,0},... | collective-permute-start | bytes 3145736 | tf_op jit(solution)/shard_map/ppermute | solution.py:308
  66.7 3.6 %mixer.1 = (bf16[4,384,256]{2,1,0:T(8,128)(2,1)S(1)}, bf16[4,384,256]{2,1,0:T(8,128)(2,1)S(1)}) custom-call(bf16[4,400,256]{2,1,0:T(8,128)(2,1)S(1)} %pad_maximum_fusion.mine_ref, bf16[4,400,256]{2,1,0:T(8,128)(2,1)S(1)} %copy-done.1, bf16[8,8,32,256]{3,2,1,0:T(8,128)(2,1)S(1)} %bitcast.15, f32[1,128]{1,0:T(1,128)S(1)} %bitcast.16), custom_call_target="tpu_custom_call" | custom-call | flops 4000000000 | bytes 4000000 | tf_op jit(solution)/shard_map/mixer/pallas_call | solution.py:249
  70.3 2.3 %collective-permute-start.4 = (bf16[4,384,256]{2,1,0:T(8,128)(2,1)S(1)}, bf16[4,384,256]{2,1,0:T(8,128)(2,1)S(1)}, u32[]{:S(2)}, u32[]{:S(2)}) collective-permute-start(bf16[4,384,256]{2,1,0:T(8,128)(2,1)S(1)} %get-tuple-element.15), channel_id=1, source_target_pairs={{0,1},{1,0},{2,3},{3,2},{4,5},{5,4},{6,7},{7,6},{8,9},{9,8},{10,11... | collective-permute-start | bytes 2359304 | tf_op jit(solution)/shard_map/ppermute | solution.py:54
  72.7 2.2 %collective-permute-start.7 = (bf16[8,32,2048]{2,1,0:T(8,128)(2,1)S(1)}, bf16[8,32,2048]{2,1,0:T(8,128)(2,1)}, u32[]{:S(2)}, u32[]{:S(2)}) collective-permute-start(bf16[8,32,2048]{2,1,0:T(8,128)(2,1)S(1)} %get-tuple-element.18.refs_0_), channel_id=1, source_target_pairs={{0,8},{1,65},{2,10},{3,67},{4,12},{5,69},{6,14},{7,71},{8,16},{9,7... | collective-permute-start | bytes 3145736 | tf_op jit(solution)/shard_map/ppermute | solution.py:311
  76.9 4.6 %collective-permute-start.8 = (bf16[8,32,2048]{2,1,0:T(8,128)(2,1)}, bf16[8,32,2048]{2,1,0:T(8,128)(2,1)}, u32[]{:S(2)}, u32[]{:S(2)}) collective-permute-start(bf16[8,32,2048]{2,1,0:T(8,128)(2,1)} %collective-permute-done.6.refs_1_), channel_id=1, source_target_pairs={{0,56},{1,449},{2,58},{3,451},{4,60},{5,453},{6,62},{7,455},{8,0},... | collective-permute-start | bytes 3145736 | tf_op jit(solution)/shard_map/ppermute | solution.py:308
  82.5 3.5 %all-to-all-start.2 = ((bf16[4,384,256]{2,1,0:T(8,128)(2,1)}), bf16[4,384,256]{2,1,0:T(8,128)(2,1)S(1)}, u32[]{:S(2)}, u32[]{:S(2)}) async-start(bf16[4,384,256]{2,1,0:T(8,128)(2,1)} %add_convert_fusion.1), calls=%async_computation.2 | async-start | bytes 1572864 | tf_op jit(solution)/shard_map/all_to_all | solution.py:74
  86.0 3.8 %collective-permute-done.7.refs_2_ = bf16[8,32,2048]{2,1,0:T(8,128)(2,1)} collective-permute-done((bf16[8,32,2048]{2,1,0:T(8,128)(2,1)S(1)}, bf16[8,32,2048]{2,1,0:T(8,128)(2,1)}, u32[]{:S(2)}, u32[]{:S(2)}) %collective-permute-start.7) | collective-permute-done | bytes 1048608 | tf_op jit(solution)/shard_map/ppermute | solution.py:311
  93.5 5.2 %collective-permute-start.10 = (bf16[8,32,2048]{2,1,0:T(8,128)(2,1)}, bf16[8,32,2048]{2,1,0:T(8,128)(2,1)}, u32[]{:S(2)}, u32[]{:S(2)}) collective-permute-start(bf16[8,32,2048]{2,1,0:T(8,128)(2,1)} %collective-permute-done.8.refs_3_), channel_id=1, source_target_pairs={{0,56},{1,449},{2,58},{3,451},{4,60},{5,453},{6,62},{7,455},{8,0},... | collective-permute-start | bytes 3145736 | tf_op jit(solution)/shard_map/ppermute | solution.py:308
  99.9 3.5 %all-to-all-start.3 = ((bf16[4,384,256]{2,1,0:T(8,128)(2,1)}), bf16[4,384,256]{2,1,0:T(8,128)(2,1)S(1)}, u32[]{:S(2)}, u32[]{:S(2)}) async-start(bf16[4,384,256]{2,1,0:T(8,128)(2,1)} %broadcast_in_dim.16), calls=%async_computation.3 | async-start | bytes 1572864 | tf_op jit(solution)/shard_map/all_to_all | solution.py:59
  103.4 3.7 %collective-permute-done.9.refs_4_ = bf16[8,32,2048]{2,1,0:T(8,128)(2,1)} collective-permute-done((bf16[8,32,2048]{2,1,0:T(8,128)(2,1)}, bf16[8,32,2048]{2,1,0:T(8,128)(2,1)}, u32[]{:S(2)}, u32[]{:S(2)}) %collective-permute-start.9) | collective-permute-done | bytes 1048608 | tf_op jit(solution)/shard_map/ppermute | solution.py:311
  110.7 5.2 %collective-permute-start.12 = (bf16[8,32,2048]{2,1,0:T(8,128)(2,1)}, bf16[8,32,2048]{2,1,0:T(8,128)(2,1)}, u32[]{:S(2)}, u32[]{:S(2)}) collective-permute-start(bf16[8,32,2048]{2,1,0:T(8,128)(2,1)} %collective-permute-done.10.refs_5_), channel_id=1, source_target_pairs={{0,56},{1,449},{2,58},{3,451},{4,60},{5,453},{6,62},{7,455},{8,0},... | collective-permute-start | bytes 3145736 | tf_op jit(solution)/shard_map/ppermute | solution.py:308
  116.0 5.4 %collective-permute-start.5 = (bf16[4,384,256]{2,1,0:T(8,128)(2,1)S(1)}, bf16[4,384,256]{2,1,0:T(8,128)(2,1)S(1)}, u32[]{:S(2)}, u32[]{:S(2)}) collective-permute-start(bf16[4,384,256]{2,1,0:T(8,128)(2,1)S(1)} %all-to-all-done.3.mix_ref), channel_id=1, source_target_pairs={{0,1},{1,0},{2,3},{3,2},{4,5},{5,4},{6,7},{7,6},{8,9},{9,8},{10,11... | collective-permute-start | bytes 2359304 | tf_op jit(solution)/shard_map/ppermute | solution.py:54
  128.0 7.1 %feed_forward.1 = (bf16[4,384,256]{2,1,0:T(8,128)(2,1)S(1)}, bf16[4,384,256]{2,1,0:T(8,128)(2,1)S(1)}) custom-call(bf16[384,2048]{1,0:T(8,128)(2,1)S(1)} %get-tuple-element.17.mid_ref, bf16[8,32,2048]{2,1,0:T(8,128)(2,1)S(1)} %get-tuple-element.18.refs_0_, bf16[8,32,2048]{2,1,0:T(8,128)(2,1)} %collective-permute-done.6.refs_1_, ...), custom_call_target="tpu_custom_call" | custom-call | flops 6000000000 | bytes 12000000 | tf_op jit(solution)/shard_map/feed_forward/pallas_call | solution.py:281
  135.1 6.0 %collective-permute-start.13 = (bf16[4,384,256]{2,1,0:T(8,128)(2,1)S(1)}, bf16[4,384,256]{2,1,0:T(8,128)(2,1)S(1)}, u32[]{:S(2)}, u32[]{:S(2)}) collective-permute-start(bf16[4,384,256]{2,1,0:T(8,128)(2,1)S(1)} %get-tuple-element.20), channel_id=1, source_target_pairs={{0,1},{1,0},{2,3},{3,2},{4,5},{5,4},{6,7},{7,6},{8,9},{9,8},{10,11... | collective-permute-start | bytes 2359304 | tf_op jit(solution)/shard_map/ppermute | solution.py:54
  143.1 14.2 %all_to_all.31 = bf16[4,384,256]{2,1,0:T(8,128)(2,1)S(1)} all-to-all(bf16[4,384,256]{2,1,0:T(8,128)(2,1)S(1)} %add_convert_fusion), channel_id=1, replica_groups=mesh['z'=8,'y'=8,'x'=4,'core'=2] {'x'}, dimensions={0} | all-to-all | bytes 1572864 | tf_op jit(solution)/shard_map/all_to_all | solution.py:74
  158.0 8.4 %all_to_all.32 = f32[8,1,768]{2,1,0:T(1,128)S(1)} all-to-all(f32[8,1,768]{2,1,0:T(1,128)S(1)} %broadcast_in_dim.17), channel_id=1, replica_groups=mesh['z'=8,'y'=8,'x'=4,'core'=2] {'x','core'}, dimensions={0} | all-to-all | bytes 49152 | tf_op jit(solution)/shard_map/all_to_all | solution.py:59
  (63 shorter events, 26.3 us)
Async XLA Ops:
  27.9 10.9 %copy-start.6 = (f32[256]{0:T(256)S(1)}, f32[256]{0:T(256)}, u32[]{:S(2)}) copy-start(f32[256]{0:T(256)} %param.10) | copy-start | bytes 3076
  27.9 11.0 %copy-start.7 = (f32[256]{0:T(256)S(1)}, f32[256]{0:T(256)}, u32[]{:S(2)}) copy-start(f32[256]{0:T(256)} %param.14) | copy-start | bytes 3076
  27.9 11.0 %copy-start.4 = (bf16[384,256]{1,0:T(8,128)(2,1)S(1)}, bf16[384,256]{1,0:T(8,128)(2,1)}, u32[]{:S(2)}) copy-start(bf16[384,256]{1,0:T(8,128)(2,1)} %param.9) | copy-start | bytes 589828
  29.1 36.5 %all-to-all-start.1 = ((bf16[8,256,256]{2,1,0:T(8,128)(2,1)}), bf16[8,256,256]{2,1,0:T(8,128)(2,1)S(1)}, u32[]{:S(2)}, u32[]{:S(2)}) async-start(bf16[8,256,256]{2,1,0:T(8,128)(2,1)} %get-tuple-element.13), calls=%async_computation.1 | async-start | bytes 2097152 | tf_op jit(solution)/shard_map/all_to_all | solution.py:69
  38.8 26.7 %copy-start.3 = (f32[128]{0:T(128)S(1)}, f32[128]{0:T(128)}, u32[]{:S(2)}) copy-start(f32[128]{0:T(128)} %param.12) | copy-start | bytes 1540
  39.2 9.4 %collective-permute-start.2 = (bf16[400,256]{1,0:T(8,128)(2,1)S(1)}, bf16[400,256]{1,0:T(8,128)(2,1)S(1)}, u32[]{:S(2)}, u32[]{:S(2)}) collective-permute-start(bf16[400,256]{1,0:T(8,128)(2,1)S(1)} %concatenate.10), channel_id=1, source_target_pairs={{0,6},{1,7},{2,0},{3,1},{4,2},{5,3},{6,4},{7,5},{8,14},{9,15},{10,... | collective-permute-start | bytes 614408 | tf_op jit(solution)/shard_map/ppermute | solution.py:50
  43.6 8.3 %collective-permute-start.1 = (bf16[400,256]{1,0:T(8,128)(2,1)S(1)}, bf16[400,256]{1,0:T(8,128)(2,1)S(1)}, u32[]{:S(2)}, u32[]{:S(2)}) collective-permute-start(bf16[400,256]{1,0:T(8,128)(2,1)S(1)} %concatenate.10), channel_id=1, source_target_pairs={{0,4},{1,5},{2,6},{3,7},{4,0},{5,1},{6,2},{7,3},{8,12},{9,13},{10,... | collective-permute-start | bytes 614408 | tf_op jit(solution)/shard_map/ppermute | solution.py:50
  46.0 10.3 %collective-permute-start = (bf16[400,256]{1,0:T(8,128)(2,1)S(1)}, bf16[400,256]{1,0:T(8,128)(2,1)S(1)}, u32[]{:S(2)}, u32[]{:S(2)}) collective-permute-start(bf16[400,256]{1,0:T(8,128)(2,1)S(1)} %concatenate.10), channel_id=1, source_target_pairs={{0,2},{1,3},{2,4},{3,5},{4,6},{5,7},{6,0},{7,1},{8,10},{9,11},{10,... | collective-permute-start | bytes 614408 | tf_op jit(solution)/shard_map/ppermute | solution.py:50
  56.5 8.2 %collective-permute-start.3 = (bf16[4,400,256]{2,1,0:T(8,128)(2,1)S(1)}, bf16[4,400,256]{2,1,0:T(8,128)(2,1)S(1)}, u32[]{:S(2)}, u32[]{:S(2)}) collective-permute-start(bf16[4,400,256]{2,1,0:T(8,128)(2,1)S(1)} %pad_maximum_fusion.mine_ref), channel_id=1, source_target_pairs={{0,1},{1,0},{2,3},{3,2},{4,5},{5,4},{6,7},{7,6},{8,9},{9,8},{10,11... | collective-permute-start | bytes 2457608 | tf_op jit(solution)/shard_map/ppermute | solution.py:54
  60.9 15.9 %collective-permute-start.6 = (bf16[8,32,2048]{2,1,0:T(8,128)(2,1)S(1)}, bf16[8,32,2048]{2,1,0:T(8,128)(2,1)}, u32[]{:S(2)}, u32[]{:S(2)}) collective-permute-start(bf16[8,32,2048]{2,1,0:T(8,128)(2,1)S(1)} %get-tuple-element.18.refs_0_), channel_id=1, source_target_pairs={{0,56},{1,449},{2,58},{3,451},{4,60},{5,453},{6,62},{7,455},{8,0},... | collective-permute-start | bytes 3145736 | tf_op jit(solution)/shard_map/ppermute | solution.py:308
  65.6 1.1 copy-start.1
  70.3 11.1 %collective-permute-start.4 = (bf16[4,384,256]{2,1,0:T(8,128)(2,1)S(1)}, bf16[4,384,256]{2,1,0:T(8,128)(2,1)S(1)}, u32[]{:S(2)}, u32[]{:S(2)}) collective-permute-start(bf16[4,384,256]{2,1,0:T(8,128)(2,1)S(1)} %get-tuple-element.15), channel_id=1, source_target_pairs={{0,1},{1,0},{2,3},{3,2},{4,5},{5,4},{6,7},{7,6},{8,9},{9,8},{10,11... | collective-permute-start | bytes 2359304 | tf_op jit(solution)/shard_map/ppermute | solution.py:54
  72.7 17.2 %collective-permute-start.7 = (bf16[8,32,2048]{2,1,0:T(8,128)(2,1)S(1)}, bf16[8,32,2048]{2,1,0:T(8,128)(2,1)}, u32[]{:S(2)}, u32[]{:S(2)}) collective-permute-start(bf16[8,32,2048]{2,1,0:T(8,128)(2,1)S(1)} %get-tuple-element.18.refs_0_), channel_id=1, source_target_pairs={{0,8},{1,65},{2,10},{3,67},{4,12},{5,69},{6,14},{7,71},{8,16},{9,7... | collective-permute-start | bytes 3145736 | tf_op jit(solution)/shard_map/ppermute | solution.py:311
  76.9 16.6 %collective-permute-start.8 = (bf16[8,32,2048]{2,1,0:T(8,128)(2,1)}, bf16[8,32,2048]{2,1,0:T(8,128)(2,1)}, u32[]{:S(2)}, u32[]{:S(2)}) collective-permute-start(bf16[8,32,2048]{2,1,0:T(8,128)(2,1)} %collective-permute-done.6.refs_1_), channel_id=1, source_target_pairs={{0,56},{1,449},{2,58},{3,451},{4,60},{5,453},{6,62},{7,455},{8,0},... | collective-permute-start | bytes 3145736 | tf_op jit(solution)/shard_map/ppermute | solution.py:308
  82.5 16.2 %all-to-all-start.2 = ((bf16[4,384,256]{2,1,0:T(8,128)(2,1)}), bf16[4,384,256]{2,1,0:T(8,128)(2,1)S(1)}, u32[]{:S(2)}, u32[]{:S(2)}) async-start(bf16[4,384,256]{2,1,0:T(8,128)(2,1)} %add_convert_fusion.1), calls=%async_computation.2 | async-start | bytes 1572864 | tf_op jit(solution)/shard_map/all_to_all | solution.py:74
  89.8 17.4 %collective-permute-start.9 = (bf16[8,32,2048]{2,1,0:T(8,128)(2,1)}, bf16[8,32,2048]{2,1,0:T(8,128)(2,1)}, u32[]{:S(2)}, u32[]{:S(2)}) collective-permute-start(bf16[8,32,2048]{2,1,0:T(8,128)(2,1)} %collective-permute-done.7.refs_2_), channel_id=1, source_target_pairs={{0,8},{1,65},{2,10},{3,67},{4,12},{5,69},{6,14},{7,71},{8,16},{9,7... | collective-permute-start | bytes 3145736 | tf_op jit(solution)/shard_map/ppermute | solution.py:311
  93.5 17.2 %collective-permute-start.10 = (bf16[8,32,2048]{2,1,0:T(8,128)(2,1)}, bf16[8,32,2048]{2,1,0:T(8,128)(2,1)}, u32[]{:S(2)}, u32[]{:S(2)}) collective-permute-start(bf16[8,32,2048]{2,1,0:T(8,128)(2,1)} %collective-permute-done.8.refs_3_), channel_id=1, source_target_pairs={{0,56},{1,449},{2,58},{3,451},{4,60},{5,453},{6,62},{7,455},{8,0},... | collective-permute-start | bytes 3145736 | tf_op jit(solution)/shard_map/ppermute | solution.py:308
  99.9 16.0 %all-to-all-start.3 = ((bf16[4,384,256]{2,1,0:T(8,128)(2,1)}), bf16[4,384,256]{2,1,0:T(8,128)(2,1)S(1)}, u32[]{:S(2)}, u32[]{:S(2)}) async-start(bf16[4,384,256]{2,1,0:T(8,128)(2,1)} %broadcast_in_dim.16), calls=%async_computation.3 | async-start | bytes 1572864 | tf_op jit(solution)/shard_map/all_to_all | solution.py:59
  107.2 19.1 %collective-permute-start.11 = (bf16[8,32,2048]{2,1,0:T(8,128)(2,1)}, bf16[8,32,2048]{2,1,0:T(8,128)(2,1)}, u32[]{:S(2)}, u32[]{:S(2)}) collective-permute-start(bf16[8,32,2048]{2,1,0:T(8,128)(2,1)} %collective-permute-done.9.refs_4_), channel_id=1, source_target_pairs={{0,8},{1,65},{2,10},{3,67},{4,12},{5,69},{6,14},{7,71},{8,16},{9,7... | collective-permute-start | bytes 3145736 | tf_op jit(solution)/shard_map/ppermute | solution.py:311
  110.7 17.2 %collective-permute-start.12 = (bf16[8,32,2048]{2,1,0:T(8,128)(2,1)}, bf16[8,32,2048]{2,1,0:T(8,128)(2,1)}, u32[]{:S(2)}, u32[]{:S(2)}) collective-permute-start(bf16[8,32,2048]{2,1,0:T(8,128)(2,1)} %collective-permute-done.10.refs_5_), channel_id=1, source_target_pairs={{0,56},{1,449},{2,58},{3,451},{4,60},{5,453},{6,62},{7,455},{8,0},... | collective-permute-start | bytes 3145736 | tf_op jit(solution)/shard_map/ppermute | solution.py:308
  116.0 7.3 %collective-permute-start.5 = (bf16[4,384,256]{2,1,0:T(8,128)(2,1)S(1)}, bf16[4,384,256]{2,1,0:T(8,128)(2,1)S(1)}, u32[]{:S(2)}, u32[]{:S(2)}) collective-permute-start(bf16[4,384,256]{2,1,0:T(8,128)(2,1)S(1)} %all-to-all-done.3.mix_ref), channel_id=1, source_target_pairs={{0,1},{1,0},{2,3},{3,2},{4,5},{5,4},{6,7},{7,6},{8,9},{9,8},{10,11... | collective-permute-start | bytes 2359304 | tf_op jit(solution)/shard_map/ppermute | solution.py:54
  123.3 1.1 copy-start.2
  135.1 7.9 %collective-permute-start.13 = (bf16[4,384,256]{2,1,0:T(8,128)(2,1)S(1)}, bf16[4,384,256]{2,1,0:T(8,128)(2,1)S(1)}, u32[]{:S(2)}, u32[]{:S(2)}) collective-permute-start(bf16[4,384,256]{2,1,0:T(8,128)(2,1)S(1)} %get-tuple-element.20), channel_id=1, source_target_pairs={{0,1},{1,0},{2,3},{3,2},{4,5},{5,4},{6,7},{7,6},{8,9},{9,8},{10,11... | collective-permute-start | bytes 2359304 | tf_op jit(solution)/shard_map/ppermute | solution.py:54
  157.5 9.0 %copy-start.5 = (f32[256]{0:T(256)S(1)}, f32[256]{0:T(256)}, u32[]{:S(2)}) copy-start(f32[256]{0:T(256)} %param.17) | copy-start | bytes 3076
  (1 other events, 0.9 us)

commit v3 on v2

--- a/solution.py
+++ b/solution.py
@@ -59,10 +59,6 @@
     return lax.all_to_all(
         jnp.broadcast_to(array[None], (count, *array.shape)), axis, 0, 0, tiled=True
     )
-
-
-def eight(array):
-    return jnp.broadcast_to(array[None], (8, *array.shape))
 
 
 def exchanged(blocks, groups):
@@ -216,6 +212,38 @@
     return [pl.BlockSpec(memory_space=pltpu.VMEM)] * count
 
 
+def prepare_kernel(w1_ref, w2_ref, w_in_ref, w_out_ref, blocks_ref):
+    for i in range(8):
+        blocks_ref[i, :, 0:1024] = w1_ref[...]
+        blocks_ref[i, :, 1024:2048] = w2_ref[...]
+        blocks_ref[i, :, 2048:2176] = w_in_ref[...]
+        blocks_ref[i, :, 2176:2304] = w_out_ref[...]
+
+
+def add_kernel(one_ref, other_ref, out_ref):
+    for i in range(4):
+        out_ref[i] = (one_ref[i].astype(f32) + other_ref[i].astype(f32)).astype(bf16)
+
+
+def spread_kernel(four_ref, out_ref):
+    low = four_ref[0].astype(f32) + four_ref[1].astype(f32)
+    high = four_ref[2].astype(f32) + four_ref[3].astype(f32)
+    total = (low + high).astype(bf16)
+    for i in range(4):
+        out_ref[i] = total
+
+
+def small_kernel(kernel, shape, *operands):
+    return pl.pallas_call(
+        kernel,
+        out_shape=jax.ShapeDtypeStruct(shape, bf16),
+        in_specs=vmem(len(operands)),
+        out_specs=vmem(1)[0],
+        compiler_params=pltpu.CompilerParams(vmem_limit_bytes=8 * MEBI),
+        cost_estimate=pl.CostEstimate(flops=1_000_000, bytes_accessed=2_000_000, transcendentals=0),
+    )(*operands)
+
+
 def split_kernel(first_ref, chunk_ref, blocks_ref, small_ref, sems):
     small = pltpu.make_async_copy(first_ref.at[:, :, pl.ds(2048, 256)], small_ref, sems.at[0])
     chunk = pltpu.make_async_copy(first_ref.at[:, :, pl.ds(0, 2048)], chunk_ref, sems.at[1])
@@ -297,8 +325,9 @@
 def layer(tokens, gain_mixer, w_in, pool_scale, w_pool_out, gain_mid, w_ff1, w_ff2, gain_out):
     rows, width = tokens.shape
     channels = w_in.shape[1]
-    packed = jnp.concatenate([w_ff1, w_ff2, w_in, w_pool_out], axis=1)
-    first = exchanged(eight(packed), FIRST)
+    weights = (w_ff1, w_ff2, w_in, w_pool_out)
+    packed = small_kernel(prepare_kernel, (8, 32, 2304), *weights)
+    first = exchanged(packed, FIRST)
     chunk, blocks = split(first)
     small = exchanged(blocks, SECOND)
     small = small.reshape(8, 8, 32, 2 * channels)
@@ -319,8 +348,11 @@
     mine = jnp.stack(pieces)
     other = from_other_core(mine)
     keep, send = mixer(mine, other, small, pool_scale[None], rows, width, channels)
-    mixer_out = scatter_sum_tp(keep, send).astype(bf16)
-    mix = everyone(mixer_out, "x")
+    block = (4, rows, width)
+    chip = small_kernel(add_kernel, block, keep, from_other_core(send))
+    four = lax.all_to_all(chip, "x", 0, 0, tiled=True)
+    spread = small_kernel(spread_kernel, block, four)
+    mix = lax.all_to_all(spread, "x", 0, 0, tiled=True)
     mix_other = from_other_core(mix)
     full, middle = middle_of(mine, other, mix, mix_other, rows, width)
     keep, send = feed_forward(full, chunks, rows, width)

time: 168 us -> 168 us (level)
  waiting for transfers between devices: 26.2 us -> 19.2 us
  starting transfers between devices: 68.9 us -> 71.4 us
  other arithmetic: 3.98 us -> 1.77 us
  Pallas kernels: 13.7 us -> 15.9 us
  local copies, waits for them, and re-layouts: 4.6 us -> 6.62 us
  blocking collectives: 49.6 us -> 51.5 us
    all_to_all x2, waiting for transfers between devices: 0.01 us -> 8.73 us  [the longest x1 5.29 us: layer(): four = lax.all_to_all(chip, 'x', 0, 0, tiled=True)]
    ppermute x3, waiting for transfers between devices: 7.54 us -> 1.01 us  [layer(): up = lax.ppermute(up, EVERY, around(1))]
    ppermute x4, waiting for transfers between devices: 7.1 us -> 0.6 us  [layer(): down = lax.ppermute(down, EVERY, around(-1))]
    ppermute x3, waiting for transfers between devices: 7.77 us -> 3.19 us  [along_x(): return lax.ppermute(array, EVERY, pairs)]
    unnamed x17 -> x25, local copies, waits for them, and re-layouts: 3.24 us -> 6.33 us
    pallas_call x0 -> x3, Pallas kernels: none -> 2.2 us  [small_kernel(): pl.pallas_call(kernel, out_shape=jax.ShapeDtypeStruct(shape, bf16), in_sp...]
    ppermute x4, waiting for transfers between devices: 3.79 us -> 5.67 us  [from_other_core(): return lax.ppermute(array, 'core', [(0, 1), (1, 0)])]
  transfers between devices with their start and end apart: 17 -> 17, of which waited for: 10 -> 8; matrix products, arithmetic and copies ran while one was open for 2% -> 0% of each run, Pallas kernels for 3% -> 5%
where the time goes in v3:
time: 168 us; the launch traced here: 167 us
  starting transfers between devices  71.4 us (43%)
  blocking collectives  51.5 us (31%)
  waiting for transfers between devices  19.2 us (11%)
  Pallas kernels  15.9 us (9%)
  local copies, waits for them, and re-layouts  6.62 us (4%)
  other arithmetic  1.77 us (1%)
    all_to_all x1, blocking collectives, exchanged(): lax.all_to_all(blocks, EVERY, 0, 0, axis_index_groups=groups, tiled=True)  26.9 us
    ppermute x4, starting transfers between devices, from_other_core(): return lax.ppermute(array, 'core', [(0, 1), (1, 0)])  19.3 us
    ppermute x4, starting transfers between devices, layer(): down = lax.ppermute(down, EVERY, around(-1))  18.6 us
    all_to_all x1, blocking collectives, scatter_sum_tp(): four = lax.all_to_all(chip, 'x', 0, 0, tiled=True).astype(f32)  15.7 us
    all_to_all x1, starting transfers between devices, exchanged(): lax.all_to_all(blocks, EVERY, 0, 0, axis_index_groups=groups, tiled=True)  9.75 us
    ppermute x3, starting transfers between devices, along_x(): return lax.ppermute(array, EVERY, pairs)  9.33 us
    all_to_all x1, blocking collectives, everyone(): lax.all_to_all(jnp.broadcast_to(array[None], (count, *array.shape)), axis...  8.85 us
    ppermute x3, starting transfers between devices, layer(): up = lax.ppermute(up, EVERY, around(1))  7.46 us
  transfers between devices with their start and end apart: 17, of which 8 were waited for; matrix products, arithmetic and copies ran while one was open for 0% of the time, Pallas kernels for 5%

profile of v3, /device:TPU:1, one launch (start us, length us, event | category | flops | bytes accessed | tf_op | source)
XLA Modules:
  0.0 166.8 jit_solution(7644702862595952416)
XLA Ops:
  3.2 26.9 %all_to_all.30.first_ref = bf16[8,32,2304]{2,1,0:T(8,128)(2,1)S(1)} all-to-all(bf16[8,32,2304]{2,1,0:T(8,128)(2,1)S(1)} %shard_map.91), channel_id=1, replica_groups={{0,64,128,192,256,320,384,448},{2,66,130,194,258,322,386,450},{4,68,132..., dimensions={0} | all-to-all | bytes 2359296 | tf_op jit(solution)/shard_map/all_to_all | solution.py:65
  31.2 9.8 %all-to-all-start.1 = ((bf16[8,256,256]{2,1,0:T(8,128)(2,1)}), bf16[8,256,256]{2,1,0:T(8,128)(2,1)S(1)}, u32[]{:S(2)}, u32[]{:S(2)}) async-start(bf16[8,256,256]{2,1,0:T(8,128)(2,1)} %get-tuple-element.13), calls=%async_computation.1 | async-start | bytes 2097152 | tf_op jit(solution)/shard_map/all_to_all | solution.py:65
  41.4 4.4 %collective-permute-start.2 = (bf16[400,256]{1,0:T(8,128)(2,1)S(1)}, bf16[400,256]{1,0:T(8,128)(2,1)S(1)}, u32[]{:S(2)}, u32[]{:S(2)}) collective-permute-start(bf16[400,256]{1,0:T(8,128)(2,1)S(1)} %concatenate.7), channel_id=1, source_target_pairs={{0,6},{1,7},{2,0},{3,1},{4,2},{5,3},{6,4},{7,5},{8,14},{9,15},{10,... | collective-permute-start | bytes 614408 | tf_op jit(solution)/shard_map/ppermute | solution.py:50
  45.8 2.4 %collective-permute-start.1 = (bf16[400,256]{1,0:T(8,128)(2,1)S(1)}, bf16[400,256]{1,0:T(8,128)(2,1)S(1)}, u32[]{:S(2)}, u32[]{:S(2)}) collective-permute-start(bf16[400,256]{1,0:T(8,128)(2,1)S(1)} %concatenate.7), channel_id=1, source_target_pairs={{0,4},{1,5},{2,6},{3,7},{4,0},{5,1},{6,2},{7,3},{8,12},{9,13},{10,... | collective-permute-start | bytes 614408 | tf_op jit(solution)/shard_map/ppermute | solution.py:50
  48.2 2.5 %collective-permute-start = (bf16[400,256]{1,0:T(8,128)(2,1)S(1)}, bf16[400,256]{1,0:T(8,128)(2,1)S(1)}, u32[]{:S(2)}, u32[]{:S(2)}) collective-permute-start(bf16[400,256]{1,0:T(8,128)(2,1)S(1)} %concatenate.7), channel_id=1, source_target_pairs={{0,2},{1,3},{2,4},{3,5},{4,6},{5,7},{6,0},{7,1},{8,10},{9,11},{10,... | collective-permute-start | bytes 614408 | tf_op jit(solution)/shard_map/ppermute | solution.py:50
  50.7 4.6 %collective-permute-start.6 = (bf16[8,32,2048]{2,1,0:T(8,128)(2,1)S(1)}, bf16[8,32,2048]{2,1,0:T(8,128)(2,1)}, u32[]{:S(2)}, u32[]{:S(2)}) collective-permute-start(bf16[8,32,2048]{2,1,0:T(8,128)(2,1)S(1)} %get-tuple-element.18.refs_0_), channel_id=1, source_target_pairs={{0,56},{1,449},{2,58},{3,451},{4,60},{5,453},{6,62},{7,455},{8,0},... | collective-permute-start | bytes 3145736 | tf_op jit(solution)/shard_map/ppermute | solution.py:337
  55.3 3.2 %collective-permute-done = bf16[400,256]{1,0:T(8,128)(2,1)S(1)} collective-permute-done((bf16[400,256]{1,0:T(8,128)(2,1)S(1)}, bf16[400,256]{1,0:T(8,128)(2,1)S(1)}, u32[]{:S(2)}, u32[]{:S(2)}) %collective-permute-start) | collective-permute-done | bytes 204832 | tf_op jit(solution)/shard_map/ppermute | solution.py:50
  58.6 4.4 %collective-permute-start.3 = (bf16[4,400,256]{2,1,0:T(8,128)(2,1)S(1)}, bf16[4,400,256]{2,1,0:T(8,128)(2,1)S(1)}, u32[]{:S(2)}, u32[]{:S(2)}) collective-permute-start(bf16[4,400,256]{2,1,0:T(8,128)(2,1)S(1)} %pad_maximum_fusion.mine_ref), channel_id=1, source_target_pairs={{0,1},{1,0},{2,3},{3,2},{4,5},{5,4},{6,7},{7,6},{8,9},{9,8},{10,11... | collective-permute-start | bytes 2457608 | tf_op jit(solution)/shard_map/ppermute | solution.py:54
  63.1 3.4 %collective-permute-start.7 = (bf16[8,32,2048]{2,1,0:T(8,128)(2,1)S(1)}, bf16[8,32,2048]{2,1,0:T(8,128)(2,1)}, u32[]{:S(2)}, u32[]{:S(2)}) collective-permute-start(bf16[8,32,2048]{2,1,0:T(8,128)(2,1)S(1)} %get-tuple-element.18.refs_0_), channel_id=1, source_target_pairs={{0,8},{1,65},{2,10},{3,67},{4,12},{5,69},{6,14},{7,71},{8,16},{9,7... | collective-permute-start | bytes 3145736 | tf_op jit(solution)/shard_map/ppermute | solution.py:340
  67.0 5.1 %collective-permute-start.8 = (bf16[8,32,2048]{2,1,0:T(8,128)(2,1)}, bf16[8,32,2048]{2,1,0:T(8,128)(2,1)}, u32[]{:S(2)}, u32[]{:S(2)}) collective-permute-start(bf16[8,32,2048]{2,1,0:T(8,128)(2,1)} %collective-permute-done.6.refs_1_), channel_id=1, source_target_pairs={{0,56},{1,449},{2,58},{3,451},{4,60},{5,453},{6,62},{7,455},{8,0},... | collective-permute-start | bytes 3145736 | tf_op jit(solution)/shard_map/ppermute | solution.py:337
  74.2 3.6 %mixer.1 = (bf16[4,384,256]{2,1,0:T(8,128)(2,1)S(1)}, bf16[4,384,256]{2,1,0:T(8,128)(2,1)S(1)}) custom-call(bf16[4,400,256]{2,1,0:T(8,128)(2,1)S(1)} %pad_maximum_fusion.mine_ref, bf16[4,400,256]{2,1,0:T(8,128)(2,1)S(1)} %copy-done.5, bf16[8,8,32,256]{3,2,1,0:T(8,128)(2,1)S(1)} %bitcast.13, f32[1,128]{1,0:T(1,128)S(1)} %bitcast.14), custom_call_target="tpu_custom_call" | custom-call | flops 4000000000 | bytes 4000000 | tf_op jit(solution)/shard_map/mixer/pallas_call | solution.py:277
  77.9 6.9 %collective-permute-start.4 = (bf16[4,384,256]{2,1,0:T(8,128)(2,1)S(1)}, bf16[4,384,256]{2,1,0:T(8,128)(2,1)S(1)}, u32[]{:S(2)}, u32[]{:S(2)}) collective-permute-start(bf16[4,384,256]{2,1,0:T(8,128)(2,1)S(1)} %get-tuple-element.15), channel_id=1, source_target_pairs={{0,1},{1,0},{2,3},{3,2},{4,5},{5,4},{6,7},{7,6},{8,9},{9,8},{10,11... | collective-permute-start | bytes 2359304 | tf_op jit(solution)/shard_map/ppermute | solution.py:54
  87.7 3.5 %all-to-all-start.2 = ((bf16[4,384,256]{2,1,0:T(8,128)(2,1)}), bf16[4,384,256]{2,1,0:T(8,128)(2,1)S(1)}, u32[]{:S(2)}, u32[]{:S(2)}) async-start(bf16[4,384,256]{2,1,0:T(8,128)(2,1)} %shard_map.92), calls=%async_computation.2 | async-start | bytes 1572864 | tf_op jit(solution)/shard_map/all_to_all | solution.py:353
  91.2 2.2 %collective-permute-start.9 = (bf16[8,32,2048]{2,1,0:T(8,128)(2,1)}, bf16[8,32,2048]{2,1,0:T(8,128)(2,1)}, u32[]{:S(2)}, u32[]{:S(2)}) collective-permute-start(bf16[8,32,2048]{2,1,0:T(8,128)(2,1)} %collective-permute-done.7.refs_2_), channel_id=1, source_target_pairs={{0,8},{1,65},{2,10},{3,67},{4,12},{5,69},{6,14},{7,71},{8,16},{9,7... | collective-permute-start | bytes 3145736 | tf_op jit(solution)/shard_map/ppermute | solution.py:340
  93.4 4.3 %collective-permute-start.10 = (bf16[8,32,2048]{2,1,0:T(8,128)(2,1)}, bf16[8,32,2048]{2,1,0:T(8,128)(2,1)}, u32[]{:S(2)}, u32[]{:S(2)}) collective-permute-start(bf16[8,32,2048]{2,1,0:T(8,128)(2,1)} %collective-permute-done.8.refs_3_), channel_id=1, source_target_pairs={{0,56},{1,449},{2,58},{3,451},{4,60},{5,453},{6,62},{7,455},{8,0},... | collective-permute-start | bytes 3145736 | tf_op jit(solution)/shard_map/ppermute | solution.py:337
  97.7 5.3 %all-to-all-done.2.four_ref = bf16[4,384,256]{2,1,0:T(8,128)(2,1)S(1)} async-done(((bf16[4,384,256]{2,1,0:T(8,128)(2,1)}), bf16[4,384,256]{2,1,0:T(8,128)(2,1)S(1)}, u32[]{:S(2)}, u32[]{:S(2)}) %all-to-all-start.2) | async-done | bytes 786464 | tf_op jit(solution)/shard_map/all_to_all | solution.py:353
  104.1 3.5 %all-to-all-start.3 = ((bf16[4,384,256]{2,1,0:T(8,128)(2,1)}), bf16[4,384,256]{2,1,0:T(8,128)(2,1)S(1)}, u32[]{:S(2)}, u32[]{:S(2)}) async-start(bf16[4,384,256]{2,1,0:T(8,128)(2,1)} %shard_map.93), calls=%async_computation.3 | async-start | bytes 1572864 | tf_op jit(solution)/shard_map/all_to_all | solution.py:355
  110.5 4.6 %collective-permute-start.12 = (bf16[8,32,2048]{2,1,0:T(8,128)(2,1)}, bf16[8,32,2048]{2,1,0:T(8,128)(2,1)}, u32[]{:S(2)}, u32[]{:S(2)}) collective-permute-start(bf16[8,32,2048]{2,1,0:T(8,128)(2,1)} %collective-permute-done.10.refs_5_), channel_id=1, source_target_pairs={{0,56},{1,449},{2,58},{3,451},{4,60},{5,453},{6,62},{7,455},{8,0},... | collective-permute-start | bytes 3145736 | tf_op jit(solution)/shard_map/ppermute | solution.py:337
  115.1 3.4 %all-to-all-done.3.mix_ref = bf16[4,384,256]{2,1,0:T(8,128)(2,1)S(1)} async-done(((bf16[4,384,256]{2,1,0:T(8,128)(2,1)}), bf16[4,384,256]{2,1,0:T(8,128)(2,1)S(1)}, u32[]{:S(2)}, u32[]{:S(2)}) %all-to-all-start.3) | async-done | bytes 786464 | tf_op jit(solution)/shard_map/all_to_all | solution.py:355
  118.5 4.1 %collective-permute-start.5 = (bf16[4,384,256]{2,1,0:T(8,128)(2,1)S(1)}, bf16[4,384,256]{2,1,0:T(8,128)(2,1)S(1)}, u32[]{:S(2)}, u32[]{:S(2)}) collective-permute-start(bf16[4,384,256]{2,1,0:T(8,128)(2,1)S(1)} %all-to-all-done.3.mix_ref), channel_id=1, source_target_pairs={{0,1},{1,0},{2,3},{3,2},{4,5},{5,4},{6,7},{7,6},{8,9},{9,8},{10,11... | collective-permute-start | bytes 2359304 | tf_op jit(solution)/shard_map/ppermute | solution.py:54
  127.6 7.1 %feed_forward.1 = (bf16[4,384,256]{2,1,0:T(8,128)(2,1)S(1)}, bf16[4,384,256]{2,1,0:T(8,128)(2,1)S(1)}) custom-call(bf16[384,2048]{1,0:T(8,128)(2,1)S(1)} %get-tuple-element.17.mid_ref, bf16[8,32,2048]{2,1,0:T(8,128)(2,1)S(1)} %get-tuple-element.18.refs_0_, bf16[8,32,2048]{2,1,0:T(8,128)(2,1)} %collective-permute-done.6.refs_1_, ...), custom_call_target="tpu_custom_call" | custom-call | flops 6000000000 | bytes 12000000 | tf_op jit(solution)/shard_map/feed_forward/pallas_call | solution.py:309
  134.7 3.9 %collective-permute-start.13 = (bf16[4,384,256]{2,1,0:T(8,128)(2,1)S(1)}, bf16[4,384,256]{2,1,0:T(8,128)(2,1)S(1)}, u32[]{:S(2)}, u32[]{:S(2)}) collective-permute-start(bf16[4,384,256]{2,1,0:T(8,128)(2,1)S(1)} %get-tuple-element.20), channel_id=1, source_target_pairs={{0,1},{1,0},{2,3},{3,2},{4,5},{5,4},{6,7},{7,6},{8,9},{9,8},{10,11... | collective-permute-start | bytes 2359304 | tf_op jit(solution)/shard_map/ppermute | solution.py:54
  140.7 15.7 %all_to_all.31 = bf16[4,384,256]{2,1,0:T(8,128)(2,1)S(1)} all-to-all(bf16[4,384,256]{2,1,0:T(8,128)(2,1)S(1)} %add_convert_fusion), channel_id=1, replica_groups=mesh['z'=8,'y'=8,'x'=4,'core'=2] {'x'}, dimensions={0} | all-to-all | bytes 1572864 | tf_op jit(solution)/shard_map/all_to_all | solution.py:70
  157.0 8.8 %all_to_all.32 = f32[8,1,768]{2,1,0:T(1,128)S(1)} all-to-all(f32[8,1,768]{2,1,0:T(1,128)S(1)} %broadcast_in_dim.8), channel_id=1, replica_groups=mesh['z'=8,'y'=8,'x'=4,'core'=2] {'x','core'}, dimensions={0} | all-to-all | bytes 49152 | tf_op jit(solution)/shard_map/all_to_all | solution.py:59
  (68 shorter events, 22.8 us)
Async XLA Ops:
  30.1 10.9 %copy-start.10 = (f32[256]{0:T(256)S(1)}, f32[256]{0:T(256)}, u32[]{:S(2)}) copy-start(f32[256]{0:T(256)} %param.10) | copy-start | bytes 3076
  30.1 11.0 %copy-start.11 = (f32[256]{0:T(256)S(1)}, f32[256]{0:T(256)}, u32[]{:S(2)}) copy-start(f32[256]{0:T(256)} %param.14) | copy-start | bytes 3076
  30.1 11.0 %copy-start.8 = (bf16[384,256]{1,0:T(8,128)(2,1)S(1)}, bf16[384,256]{1,0:T(8,128)(2,1)}, u32[]{:S(2)}) copy-start(bf16[384,256]{1,0:T(8,128)(2,1)} %param.9) | copy-start | bytes 589828
  31.2 41.9 %all-to-all-start.1 = ((bf16[8,256,256]{2,1,0:T(8,128)(2,1)}), bf16[8,256,256]{2,1,0:T(8,128)(2,1)S(1)}, u32[]{:S(2)}, u32[]{:S(2)}) async-start(bf16[8,256,256]{2,1,0:T(8,128)(2,1)} %get-tuple-element.13), calls=%async_computation.1 | async-start | bytes 2097152 | tf_op jit(solution)/shard_map/all_to_all | solution.py:65
  41.0 32.1 %copy-start.7 = (f32[128]{0:T(128)S(1)}, f32[128]{0:T(128)}, u32[]{:S(2)}) copy-start(f32[128]{0:T(128)} %param.12) | copy-start | bytes 1540
  41.4 13.9 %collective-permute-start.2 = (bf16[400,256]{1,0:T(8,128)(2,1)S(1)}, bf16[400,256]{1,0:T(8,128)(2,1)S(1)}, u32[]{:S(2)}, u32[]{:S(2)}) collective-permute-start(bf16[400,256]{1,0:T(8,128)(2,1)S(1)} %concatenate.7), channel_id=1, source_target_pairs={{0,6},{1,7},{2,0},{3,1},{4,2},{5,3},{6,4},{7,5},{8,14},{9,15},{10,... | collective-permute-start | bytes 614408 | tf_op jit(solution)/shard_map/ppermute | solution.py:50
  45.8 9.5 %collective-permute-start.1 = (bf16[400,256]{1,0:T(8,128)(2,1)S(1)}, bf16[400,256]{1,0:T(8,128)(2,1)S(1)}, u32[]{:S(2)}, u32[]{:S(2)}) collective-permute-start(bf16[400,256]{1,0:T(8,128)(2,1)S(1)} %concatenate.7), channel_id=1, source_target_pairs={{0,4},{1,5},{2,6},{3,7},{4,0},{5,1},{6,2},{7,3},{8,12},{9,13},{10,... | collective-permute-start | bytes 614408 | tf_op jit(solution)/shard_map/ppermute | solution.py:50
  48.2 10.3 %collective-permute-start = (bf16[400,256]{1,0:T(8,128)(2,1)S(1)}, bf16[400,256]{1,0:T(8,128)(2,1)S(1)}, u32[]{:S(2)}, u32[]{:S(2)}) collective-permute-start(bf16[400,256]{1,0:T(8,128)(2,1)S(1)} %concatenate.7), channel_id=1, source_target_pairs={{0,2},{1,3},{2,4},{3,5},{4,6},{5,7},{6,0},{7,1},{8,10},{9,11},{10,... | collective-permute-start | bytes 614408 | tf_op jit(solution)/shard_map/ppermute | solution.py:50
  50.7 16.3 %collective-permute-start.6 = (bf16[8,32,2048]{2,1,0:T(8,128)(2,1)S(1)}, bf16[8,32,2048]{2,1,0:T(8,128)(2,1)}, u32[]{:S(2)}, u32[]{:S(2)}) collective-permute-start(bf16[8,32,2048]{2,1,0:T(8,128)(2,1)S(1)} %get-tuple-element.18.refs_0_), channel_id=1, source_target_pairs={{0,56},{1,449},{2,58},{3,451},{4,60},{5,453},{6,62},{7,455},{8,0},... | collective-permute-start | bytes 3145736 | tf_op jit(solution)/shard_map/ppermute | solution.py:337
  58.6 13.5 %collective-permute-start.3 = (bf16[4,400,256]{2,1,0:T(8,128)(2,1)S(1)}, bf16[4,400,256]{2,1,0:T(8,128)(2,1)S(1)}, u32[]{:S(2)}, u32[]{:S(2)}) collective-permute-start(bf16[4,400,256]{2,1,0:T(8,128)(2,1)S(1)} %pad_maximum_fusion.mine_ref), channel_id=1, source_target_pairs={{0,1},{1,0},{2,3},{3,2},{4,5},{5,4},{6,7},{7,6},{8,9},{9,8},{10,11... | collective-permute-start | bytes 2457608 | tf_op jit(solution)/shard_map/ppermute | solution.py:54
  63.1 28.1 %collective-permute-start.7 = (bf16[8,32,2048]{2,1,0:T(8,128)(2,1)S(1)}, bf16[8,32,2048]{2,1,0:T(8,128)(2,1)}, u32[]{:S(2)}, u32[]{:S(2)}) collective-permute-start(bf16[8,32,2048]{2,1,0:T(8,128)(2,1)S(1)} %get-tuple-element.18.refs_0_), channel_id=1, source_target_pairs={{0,8},{1,65},{2,10},{3,67},{4,12},{5,69},{6,14},{7,71},{8,16},{9,7... | collective-permute-start | bytes 3145736 | tf_op jit(solution)/shard_map/ppermute | solution.py:340
  67.0 26.4 %collective-permute-start.8 = (bf16[8,32,2048]{2,1,0:T(8,128)(2,1)}, bf16[8,32,2048]{2,1,0:T(8,128)(2,1)}, u32[]{:S(2)}, u32[]{:S(2)}) collective-permute-start(bf16[8,32,2048]{2,1,0:T(8,128)(2,1)} %collective-permute-done.6.refs_1_), channel_id=1, source_target_pairs={{0,56},{1,449},{2,58},{3,451},{4,60},{5,453},{6,62},{7,455},{8,0},... | collective-permute-start | bytes 3145736 | tf_op jit(solution)/shard_map/ppermute | solution.py:337
  73.1 1.1 copy-start.5
  77.9 8.7 %collective-permute-start.4 = (bf16[4,384,256]{2,1,0:T(8,128)(2,1)S(1)}, bf16[4,384,256]{2,1,0:T(8,128)(2,1)S(1)}, u32[]{:S(2)}, u32[]{:S(2)}) collective-permute-start(bf16[4,384,256]{2,1,0:T(8,128)(2,1)S(1)} %get-tuple-element.15), channel_id=1, source_target_pairs={{0,1},{1,0},{2,3},{3,2},{4,5},{5,4},{6,7},{7,6},{8,9},{9,8},{10,11... | collective-permute-start | bytes 2359304 | tf_op jit(solution)/shard_map/ppermute | solution.py:54
  87.7 15.3 %all-to-all-start.2 = ((bf16[4,384,256]{2,1,0:T(8,128)(2,1)}), bf16[4,384,256]{2,1,0:T(8,128)(2,1)S(1)}, u32[]{:S(2)}, u32[]{:S(2)}) async-start(bf16[4,384,256]{2,1,0:T(8,128)(2,1)} %shard_map.92), calls=%async_computation.2 | async-start | bytes 1572864 | tf_op jit(solution)/shard_map/all_to_all | solution.py:353
  91.2 17.4 %collective-permute-start.9 = (bf16[8,32,2048]{2,1,0:T(8,128)(2,1)}, bf16[8,32,2048]{2,1,0:T(8,128)(2,1)}, u32[]{:S(2)}, u32[]{:S(2)}) collective-permute-start(bf16[8,32,2048]{2,1,0:T(8,128)(2,1)} %collective-permute-done.7.refs_2_), channel_id=1, source_target_pairs={{0,8},{1,65},{2,10},{3,67},{4,12},{5,69},{6,14},{7,71},{8,16},{9,7... | collective-permute-start | bytes 3145736 | tf_op jit(solution)/shard_map/ppermute | solution.py:340
  93.4 17.1 %collective-permute-start.10 = (bf16[8,32,2048]{2,1,0:T(8,128)(2,1)}, bf16[8,32,2048]{2,1,0:T(8,128)(2,1)}, u32[]{:S(2)}, u32[]{:S(2)}) collective-permute-start(bf16[8,32,2048]{2,1,0:T(8,128)(2,1)} %collective-permute-done.8.refs_3_), channel_id=1, source_target_pairs={{0,56},{1,449},{2,58},{3,451},{4,60},{5,453},{6,62},{7,455},{8,0},... | collective-permute-start | bytes 3145736 | tf_op jit(solution)/shard_map/ppermute | solution.py:337
  104.1 14.5 %all-to-all-start.3 = ((bf16[4,384,256]{2,1,0:T(8,128)(2,1)}), bf16[4,384,256]{2,1,0:T(8,128)(2,1)S(1)}, u32[]{:S(2)}, u32[]{:S(2)}) async-start(bf16[4,384,256]{2,1,0:T(8,128)(2,1)} %shard_map.93), calls=%async_computation.3 | async-start | bytes 1572864 | tf_op jit(solution)/shard_map/all_to_all | solution.py:355
  108.6 19.0 %collective-permute-start.11 = (bf16[8,32,2048]{2,1,0:T(8,128)(2,1)}, bf16[8,32,2048]{2,1,0:T(8,128)(2,1)}, u32[]{:S(2)}, u32[]{:S(2)}) collective-permute-start(bf16[8,32,2048]{2,1,0:T(8,128)(2,1)} %collective-permute-done.9.refs_4_), channel_id=1, source_target_pairs={{0,8},{1,65},{2,10},{3,67},{4,12},{5,69},{6,14},{7,71},{8,16},{9,7... | collective-permute-start | bytes 3145736 | tf_op jit(solution)/shard_map/ppermute | solution.py:340
  110.5 17.1 %collective-permute-start.12 = (bf16[8,32,2048]{2,1,0:T(8,128)(2,1)}, bf16[8,32,2048]{2,1,0:T(8,128)(2,1)}, u32[]{:S(2)}, u32[]{:S(2)}) collective-permute-start(bf16[8,32,2048]{2,1,0:T(8,128)(2,1)} %collective-permute-done.10.refs_5_), channel_id=1, source_target_pairs={{0,56},{1,449},{2,58},{3,451},{4,60},{5,453},{6,62},{7,455},{8,0},... | collective-permute-start | bytes 3145736 | tf_op jit(solution)/shard_map/ppermute | solution.py:337
  118.5 6.0 %collective-permute-start.5 = (bf16[4,384,256]{2,1,0:T(8,128)(2,1)S(1)}, bf16[4,384,256]{2,1,0:T(8,128)(2,1)S(1)}, u32[]{:S(2)}, u32[]{:S(2)}) collective-permute-start(bf16[4,384,256]{2,1,0:T(8,128)(2,1)S(1)} %all-to-all-done.3.mix_ref), channel_id=1, source_target_pairs={{0,1},{1,0},{2,3},{3,2},{4,5},{5,4},{6,7},{7,6},{8,9},{9,8},{10,11... | collective-permute-start | bytes 2359304 | tf_op jit(solution)/shard_map/ppermute | solution.py:54
  124.6 1.1 copy-start.6
  134.7 5.8 %collective-permute-start.13 = (bf16[4,384,256]{2,1,0:T(8,128)(2,1)S(1)}, bf16[4,384,256]{2,1,0:T(8,128)(2,1)S(1)}, u32[]{:S(2)}, u32[]{:S(2)}) collective-permute-start(bf16[4,384,256]{2,1,0:T(8,128)(2,1)S(1)} %get-tuple-element.20), channel_id=1, source_target_pairs={{0,1},{1,0},{2,3},{3,2},{4,5},{5,4},{6,7},{7,6},{8,9},{9,8},{10,11... | collective-permute-start | bytes 2359304 | tf_op jit(solution)/shard_map/ppermute | solution.py:54
  156.6 9.4 %copy-start.9 = (f32[256]{0:T(256)S(1)}, f32[256]{0:T(256)}, u32[]{:S(2)}) copy-start(f32[256]{0:T(256)} %param.17) | copy-start | bytes 3076
  (5 other events, 4.0 us)

commit v4 on v1

--- a/solution.py
+++ b/solution.py
@@ -182,33 +182,47 @@
     chunks, (keep_ref, send_ref, hid_ref, w_ref, sems) = refs[:8], refs[8:]
     core = lax.axis_index("core")
     place = jnp.where(core == 0, lax.axis_index("y"), lax.axis_index("z"))
-    copies = [[], []]
-    for half in range(2):
-        where = pl.ds(half * 1024, 1024)
+    groups = [pl.ds(n * 256, 256) for n in range(4)] + [pl.ds(1024, 1024)]
+
+    def copies(g, along_y):
+        result = []
         for k, (chunk, offset) in enumerate(zip(chunks, OFFSETS)):
             source = lax.rem(place + (8 - offset), 8)
-            for j in range(8):
-                copy = pltpu.make_async_copy(
-                    chunk.at[j, :, where],
-                    w_ref.at[row_at(core, source, j), where],
-                    sems.at[half, k, j],
-                )
+            if along_y:
+                target = w_ref.at[:, source, :, groups[g]]
+            else:
+                target = w_ref.at[source, :, :, groups[g]]
+            result.append(
+                pltpu.make_async_copy(chunk.at[:, :, groups[g]], target, sems.at[g, k])
+            )
+        return result
+
+    @pl.when(core == 0)
+    def _():
+        for g in range(5):
+            for copy in copies(g, True):
                 copy.start()
-                copies[half].append(copy)
-    for copy in copies[0]:
-        copy.wait()
+
+    @pl.when(core == 1)
+    def _():
+        for g in range(5):
+            for copy in copies(g, False):
+                copy.start()
+
     for n in range(4):
-        where = slice(n * 256, (n + 1) * 256)
-        up = jnp.dot(mid_ref[...], w_ref[:, where], preferred_element_type=f32)
+        for copy in copies(n, False):
+            copy.wait()
+        w_up = w_ref[:, :, :, n * 256 : (n + 1) * 256].reshape(2048, 256)
+        up = jnp.dot(mid_ref[...], w_up, preferred_element_type=f32)
         up = jnp.maximum(up, 0.0)
-        hid_ref[:, where] = (up * up).astype(bf16)
-    for copy in copies[1]:
+        hid_ref[:, n * 256 : (n + 1) * 256] = (up * up).astype(bf16)
+    for copy in copies(4, False):
         copy.wait()
     for xb in range(4):
         for ref, c in ((keep_ref, core), (send_ref, 1 - core)):
             term = lax.dot_general(
                 hid_ref[...],
-                w_ref[columns_of(xb, c), 1024:],
+                w_ref[2 * xb + c, :, :, 1024:].reshape(256, 1024),
                 (((1,), (1,)), ((), ())),
                 preferred_element_type=f32,
             )
@@ -260,8 +274,8 @@
         out_specs=tuple(vmem(2)),
         scratch_shapes=[
             pltpu.VMEM((rows, 1024), bf16),
-            pltpu.VMEM((2048, 2048), bf16),
-            pltpu.SemaphoreType.DMA((2, 8, 8)),
+            pltpu.VMEM((8, 8, 32, 2048), bf16),
+            pltpu.SemaphoreType.DMA((5, 8)),
         ],
         compiler_params=pltpu.CompilerParams(vmem_limit_bytes=30 * MEBI),
         cost_estimate=pl.CostEstimate(flops=6_000_000_000, bytes_accessed=12_000_000, transcendentals=0),

time: 171 us -> 171 us (level)
  no operation moved by 1% of the time
where the time goes in v4:
time: 171 us; the launch traced here: 170 us
  starting transfers between devices  68.9 us (40%)
  blocking collectives  49.6 us (29%)
  waiting for transfers between devices  26.2 us (15%)
  Pallas kernels  12.8 us (7%)
  local copies, waits for them, and re-layouts  7.97 us (5%)
  other arithmetic  3.98 us (2%)
    all_to_all x1, blocking collectives, among(): lax.all_to_all(jnp.broadcast_to(array[None], (8, *array.shape)), EVERY, 0...  26.9 us
    ppermute x4, starting transfers between devices, layer(): down = lax.ppermute(down, EVERY, around(-1))  18.7 us
    ppermute x4, starting transfers between devices, from_other_core(): return lax.ppermute(array, 'core', [(0, 1), (1, 0)])  18.2 us
    all_to_all x1, blocking collectives, scatter_sum_tp(): four = lax.all_to_all(chip, 'x', 0, 0, tiled=True).astype(f32)  14.2 us
    all_to_all x1, starting transfers between devices, among(): lax.all_to_all(jnp.broadcast_to(array[None], (8, *array.shape)), EVERY, 0...  9.74 us
    ppermute x3, starting transfers between devices, along_x(): return lax.ppermute(array, EVERY, pairs)  9.33 us
    all_to_all x1, blocking collectives, everyone(): lax.all_to_all(jnp.broadcast_to(array[None], (count, *array.shape)), axis...  8.45 us
    ppermute x3, waiting for transfers between devices, along_x(): return lax.ppermute(array, EVERY, pairs)  7.77 us
  transfers between devices with their start and end apart: 17, of which 10 were waited for; matrix products, arithmetic and copies ran while one was open for 2% of the time, Pallas kernels for 3%

profile of v4, /device:TPU:1, one launch (start us, length us, event | category | flops | bytes accessed | tf_op | source)
XLA Modules:
  0.0 169.9 jit_solution(241118475027069424)
XLA Ops:
  1.0 26.9 %all_to_all.30 = bf16[8,32,2304]{2,1,0:T(8,128)(2,1)S(1)} all-to-all(bf16[8,32,2304]{2,1,0:T(8,128)(2,1)S(1)} %broadcast_in_dim.17), channel_id=1, replica_groups={{0,64,128,192,256,320,384,448},{2,66,130,194,258,322,386,450},{4,68,132..., dimensions={0} | all-to-all | bytes 2359296 | tf_op jit(solution)/shard_map/all_to_all | solution.py:65
  30.0 9.7 %all-to-all-start.1 = ((bf16[8,256,256]{2,1,0:T(8,128)(2,1)}), bf16[8,256,256]{2,1,0:T(8,128)(2,1)S(1)}, u32[]{:S(2)}, u32[]{:S(2)}) async-start(bf16[8,256,256]{2,1,0:T(8,128)(2,1)} %broadcast_in_dim.19), calls=%async_computation.1 | async-start | bytes 2097152 | tf_op jit(solution)/shard_map/all_to_all | solution.py:65
  40.1 4.4 %collective-permute-start.2 = (bf16[400,256]{1,0:T(8,128)(2,1)S(1)}, bf16[400,256]{1,0:T(8,128)(2,1)S(1)}, u32[]{:S(2)}, u32[]{:S(2)}) collective-permute-start(bf16[400,256]{1,0:T(8,128)(2,1)S(1)} %concatenate.10), channel_id=1, source_target_pairs={{0,6},{1,7},{2,0},{3,1},{4,2},{5,3},{6,4},{7,5},{8,14},{9,15},{10,... | collective-permute-start | bytes 614408 | tf_op jit(solution)/shard_map/ppermute | solution.py:50
  44.5 2.4 %collective-permute-start.1 = (bf16[400,256]{1,0:T(8,128)(2,1)S(1)}, bf16[400,256]{1,0:T(8,128)(2,1)S(1)}, u32[]{:S(2)}, u32[]{:S(2)}) collective-permute-start(bf16[400,256]{1,0:T(8,128)(2,1)S(1)} %concatenate.10), channel_id=1, source_target_pairs={{0,4},{1,5},{2,6},{3,7},{4,0},{5,1},{6,2},{7,3},{8,12},{9,13},{10,... | collective-permute-start | bytes 614408 | tf_op jit(solution)/shard_map/ppermute | solution.py:50
  47.0 2.5 %collective-permute-start = (bf16[400,256]{1,0:T(8,128)(2,1)S(1)}, bf16[400,256]{1,0:T(8,128)(2,1)S(1)}, u32[]{:S(2)}, u32[]{:S(2)}) collective-permute-start(bf16[400,256]{1,0:T(8,128)(2,1)S(1)} %concatenate.10), channel_id=1, source_target_pairs={{0,2},{1,3},{2,4},{3,5},{4,6},{5,7},{6,0},{7,1},{8,10},{9,11},{10,... | collective-permute-start | bytes 614408 | tf_op jit(solution)/shard_map/ppermute | solution.py:50
  49.5 3.3 %collective-permute-done.1 = bf16[400,256]{1,0:T(8,128)(2,1)S(1)} collective-permute-done((bf16[400,256]{1,0:T(8,128)(2,1)S(1)}, bf16[400,256]{1,0:T(8,128)(2,1)S(1)}, u32[]{:S(2)}, u32[]{:S(2)}) %collective-permute-start.1) | collective-permute-done | bytes 204832 | tf_op jit(solution)/shard_map/ppermute | solution.py:50
  52.8 4.4 %collective-permute-done = bf16[400,256]{1,0:T(8,128)(2,1)S(1)} collective-permute-done((bf16[400,256]{1,0:T(8,128)(2,1)S(1)}, bf16[400,256]{1,0:T(8,128)(2,1)S(1)}, u32[]{:S(2)}, u32[]{:S(2)}) %collective-permute-start) | collective-permute-done | bytes 204832 | tf_op jit(solution)/shard_map/ppermute | solution.py:50
  57.4 4.4 %collective-permute-start.3 = (bf16[4,400,256]{2,1,0:T(8,128)(2,1)S(1)}, bf16[4,400,256]{2,1,0:T(8,128)(2,1)S(1)}, u32[]{:S(2)}, u32[]{:S(2)}) collective-permute-start(bf16[4,400,256]{2,1,0:T(8,128)(2,1)S(1)} %pad_maximum_fusion.mine_ref), channel_id=1, source_target_pairs={{0,1},{1,0},{2,3},{3,2},{4,5},{5,4},{6,7},{7,6},{8,9},{9,8},{10,11... | collective-permute-start | bytes 2457608 | tf_op jit(solution)/shard_map/ppermute | solution.py:54
  63.1 3.7 %collective-permute-start.6 = (bf16[8,32,2048]{2,1,0:T(8,128)(2,1)S(1)}, bf16[8,32,2048]{2,1,0:T(8,128)(2,1)}, u32[]{:S(2)}, u32[]{:S(2)}) collective-permute-start(bf16[8,32,2048]{2,1,0:T(8,128)(2,1)S(1)} %slice.45.refs_0_), channel_id=1, source_target_pairs={{0,56},{1,449},{2,58},{3,451},{4,60},{5,453},{6,62},{7,455},{8,0},... | collective-permute-start | bytes 3145736 | tf_op jit(solution)/shard_map/ppermute | solution.py:297
  68.9 3.6 %mixer.1 = (bf16[4,384,256]{2,1,0:T(8,128)(2,1)S(1)}, bf16[4,384,256]{2,1,0:T(8,128)(2,1)S(1)}) custom-call(bf16[4,400,256]{2,1,0:T(8,128)(2,1)S(1)} %pad_maximum_fusion.mine_ref, bf16[4,400,256]{2,1,0:T(8,128)(2,1)S(1)} %copy-done.1, bf16[8,8,32,256]{3,2,1,0:T(8,128)(2,1)S(1)} %bitcast.16, f32[1,128]{1,0:T(1,128)S(1)} %bitcast.17), custom_call_target="tpu_custom_call" | custom-call | flops 4000000000 | bytes 4000000 | tf_op jit(solution)/shard_map/mixer/pallas_call | solution.py:238
  72.6 2.3 %collective-permute-start.4 = (bf16[4,384,256]{2,1,0:T(8,128)(2,1)S(1)}, bf16[4,384,256]{2,1,0:T(8,128)(2,1)S(1)}, u32[]{:S(2)}, u32[]{:S(2)}) collective-permute-start(bf16[4,384,256]{2,1,0:T(8,128)(2,1)S(1)} %get-tuple-element.12), channel_id=1, source_target_pairs={{0,1},{1,0},{2,3},{3,2},{4,5},{5,4},{6,7},{7,6},{8,9},{9,8},{10,11... | collective-permute-start | bytes 2359304 | tf_op jit(solution)/shard_map/ppermute | solution.py:54
  74.9 2.2 %collective-permute-start.7 = (bf16[8,32,2048]{2,1,0:T(8,128)(2,1)S(1)}, bf16[8,32,2048]{2,1,0:T(8,128)(2,1)}, u32[]{:S(2)}, u32[]{:S(2)}) collective-permute-start(bf16[8,32,2048]{2,1,0:T(8,128)(2,1)S(1)} %slice.45.refs_0_), channel_id=1, source_target_pairs={{0,8},{1,65},{2,10},{3,67},{4,12},{5,69},{6,14},{7,71},{8,16},{9,7... | collective-permute-start | bytes 3145736 | tf_op jit(solution)/shard_map/ppermute | solution.py:300
  79.1 4.6 %collective-permute-start.8 = (bf16[8,32,2048]{2,1,0:T(8,128)(2,1)}, bf16[8,32,2048]{2,1,0:T(8,128)(2,1)}, u32[]{:S(2)}, u32[]{:S(2)}) collective-permute-start(bf16[8,32,2048]{2,1,0:T(8,128)(2,1)} %collective-permute-done.6.refs_1_), channel_id=1, source_target_pairs={{0,56},{1,449},{2,58},{3,451},{4,60},{5,453},{6,62},{7,455},{8,0},... | collective-permute-start | bytes 3145736 | tf_op jit(solution)/shard_map/ppermute | solution.py:297
  84.8 3.5 %all-to-all-start.2 = ((bf16[4,384,256]{2,1,0:T(8,128)(2,1)}), bf16[4,384,256]{2,1,0:T(8,128)(2,1)S(1)}, u32[]{:S(2)}, u32[]{:S(2)}) async-start(bf16[4,384,256]{2,1,0:T(8,128)(2,1)} %add_convert_fusion.1), calls=%async_computation.2 | async-start | bytes 1572864 | tf_op jit(solution)/shard_map/all_to_all | solution.py:77
  88.3 3.8 %collective-permute-done.7.refs_2_ = bf16[8,32,2048]{2,1,0:T(8,128)(2,1)} collective-permute-done((bf16[8,32,2048]{2,1,0:T(8,128)(2,1)S(1)}, bf16[8,32,2048]{2,1,0:T(8,128)(2,1)}, u32[]{:S(2)}, u32[]{:S(2)}) %collective-permute-start.7) | collective-permute-done | bytes 1048608 | tf_op jit(solution)/shard_map/ppermute | solution.py:300
  95.7 5.2 %collective-permute-start.10 = (bf16[8,32,2048]{2,1,0:T(8,128)(2,1)}, bf16[8,32,2048]{2,1,0:T(8,128)(2,1)}, u32[]{:S(2)}, u32[]{:S(2)}) collective-permute-start(bf16[8,32,2048]{2,1,0:T(8,128)(2,1)} %collective-permute-done.8.refs_3_), channel_id=1, source_target_pairs={{0,56},{1,449},{2,58},{3,451},{4,60},{5,453},{6,62},{7,455},{8,0},... | collective-permute-start | bytes 3145736 | tf_op jit(solution)/shard_map/ppermute | solution.py:297
  102.2 3.5 %all-to-all-start.3 = ((bf16[4,384,256]{2,1,0:T(8,128)(2,1)}), bf16[4,384,256]{2,1,0:T(8,128)(2,1)S(1)}, u32[]{:S(2)}, u32[]{:S(2)}) async-start(bf16[4,384,256]{2,1,0:T(8,128)(2,1)} %broadcast_in_dim.43), calls=%async_computation.3 | async-start | bytes 1572864 | tf_op jit(solution)/shard_map/all_to_all | solution.py:59
  105.7 3.8 %collective-permute-done.9.refs_4_ = bf16[8,32,2048]{2,1,0:T(8,128)(2,1)} collective-permute-done((bf16[8,32,2048]{2,1,0:T(8,128)(2,1)}, bf16[8,32,2048]{2,1,0:T(8,128)(2,1)}, u32[]{:S(2)}, u32[]{:S(2)}) %collective-permute-start.9) | collective-permute-done | bytes 1048608 | tf_op jit(solution)/shard_map/ppermute | solution.py:300
  113.0 5.2 %collective-permute-start.12 = (bf16[8,32,2048]{2,1,0:T(8,128)(2,1)}, bf16[8,32,2048]{2,1,0:T(8,128)(2,1)}, u32[]{:S(2)}, u32[]{:S(2)}) collective-permute-start(bf16[8,32,2048]{2,1,0:T(8,128)(2,1)} %collective-permute-done.10.refs_5_), channel_id=1, source_target_pairs={{0,56},{1,449},{2,58},{3,451},{4,60},{5,453},{6,62},{7,455},{8,0},... | collective-permute-start | bytes 3145736 | tf_op jit(solution)/shard_map/ppermute | solution.py:297
  118.2 5.4 %collective-permute-start.5 = (bf16[4,384,256]{2,1,0:T(8,128)(2,1)S(1)}, bf16[4,384,256]{2,1,0:T(8,128)(2,1)S(1)}, u32[]{:S(2)}, u32[]{:S(2)}) collective-permute-start(bf16[4,384,256]{2,1,0:T(8,128)(2,1)S(1)} %all-to-all-done.3.mix_ref), channel_id=1, source_target_pairs={{0,1},{1,0},{2,3},{3,2},{4,5},{5,4},{6,7},{7,6},{8,9},{9,8},{10,11... | collective-permute-start | bytes 2359304 | tf_op jit(solution)/shard_map/ppermute | solution.py:54
  130.2 7.3 %feed_forward.1 = (bf16[4,384,256]{2,1,0:T(8,128)(2,1)S(1)}, bf16[4,384,256]{2,1,0:T(8,128)(2,1)S(1)}) custom-call(bf16[384,2048]{1,0:T(8,128)(2,1)S(1)} %get-tuple-element.14.mid_ref, bf16[8,32,2048]{2,1,0:T(8,128)(2,1)S(1)} %slice.45.refs_0_, bf16[8,32,2048]{2,1,0:T(8,128)(2,1)} %collective-permute-done.6.refs_1_, ...), custom_call_target="tpu_custom_call" | custom-call | flops 6000000000 | bytes 12000000 | tf_op jit(solution)/shard_map/feed_forward/pallas_call | solution.py:270
  137.6 6.0 %collective-permute-start.13 = (bf16[4,384,256]{2,1,0:T(8,128)(2,1)S(1)}, bf16[4,384,256]{2,1,0:T(8,128)(2,1)S(1)}, u32[]{:S(2)}, u32[]{:S(2)}) collective-permute-start(bf16[4,384,256]{2,1,0:T(8,128)(2,1)S(1)} %get-tuple-element.16), channel_id=1, source_target_pairs={{0,1},{1,0},{2,3},{3,2},{4,5},{5,4},{6,7},{7,6},{8,9},{9,8},{10,11... | collective-permute-start | bytes 2359304 | tf_op jit(solution)/shard_map/ppermute | solution.py:54
  145.6 14.2 %all_to_all.31 = bf16[4,384,256]{2,1,0:T(8,128)(2,1)S(1)} all-to-all(bf16[4,384,256]{2,1,0:T(8,128)(2,1)S(1)} %add_convert_fusion), channel_id=1, replica_groups=mesh['z'=8,'y'=8,'x'=4,'core'=2] {'x'}, dimensions={0} | all-to-all | bytes 1572864 | tf_op jit(solution)/shard_map/all_to_all | solution.py:77
  160.5 8.4 %all_to_all.32 = f32[8,1,768]{2,1,0:T(1,128)S(1)} all-to-all(f32[8,1,768]{2,1,0:T(1,128)S(1)} %broadcast_in_dim.44), channel_id=1, replica_groups=mesh['z'=8,'y'=8,'x'=4,'core'=2] {'x','core'}, dimensions={0} | all-to-all | bytes 49152 | tf_op jit(solution)/shard_map/all_to_all | solution.py:59
  (67 shorter events, 28.5 us)
Async XLA Ops:
  29.0 10.8 %copy-start.7 = (f32[256]{0:T(256)S(1)}, f32[256]{0:T(256)}, u32[]{:S(2)}) copy-start(f32[256]{0:T(256)} %param.10) | copy-start | bytes 3076
  29.0 10.8 %copy-start.8 = (f32[256]{0:T(256)S(1)}, f32[256]{0:T(256)}, u32[]{:S(2)}) copy-start(f32[256]{0:T(256)} %param.14) | copy-start | bytes 3076
  29.0 10.9 %copy-start.5 = (bf16[384,256]{1,0:T(8,128)(2,1)S(1)}, bf16[384,256]{1,0:T(8,128)(2,1)}, u32[]{:S(2)}) copy-start(bf16[384,256]{1,0:T(8,128)(2,1)} %param.9) | copy-start | bytes 589828
  30.0 37.8 %all-to-all-start.1 = ((bf16[8,256,256]{2,1,0:T(8,128)(2,1)}), bf16[8,256,256]{2,1,0:T(8,128)(2,1)S(1)}, u32[]{:S(2)}, u32[]{:S(2)}) async-start(bf16[8,256,256]{2,1,0:T(8,128)(2,1)} %broadcast_in_dim.19), calls=%async_computation.1 | async-start | bytes 2097152 | tf_op jit(solution)/shard_map/all_to_all | solution.py:65
  40.1 9.4 %collective-permute-start.2 = (bf16[400,256]{1,0:T(8,128)(2,1)S(1)}, bf16[400,256]{1,0:T(8,128)(2,1)S(1)}, u32[]{:S(2)}, u32[]{:S(2)}) collective-permute-start(bf16[400,256]{1,0:T(8,128)(2,1)S(1)} %concatenate.10), channel_id=1, source_target_pairs={{0,6},{1,7},{2,0},{3,1},{4,2},{5,3},{6,4},{7,5},{8,14},{9,15},{10,... | collective-permute-start | bytes 614408 | tf_op jit(solution)/shard_map/ppermute | solution.py:50
  44.5 8.3 %collective-permute-start.1 = (bf16[400,256]{1,0:T(8,128)(2,1)S(1)}, bf16[400,256]{1,0:T(8,128)(2,1)S(1)}, u32[]{:S(2)}, u32[]{:S(2)}) collective-permute-start(bf16[400,256]{1,0:T(8,128)(2,1)S(1)} %concatenate.10), channel_id=1, source_target_pairs={{0,4},{1,5},{2,6},{3,7},{4,0},{5,1},{6,2},{7,3},{8,12},{9,13},{10,... | collective-permute-start | bytes 614408 | tf_op jit(solution)/shard_map/ppermute | solution.py:50
  47.0 10.3 %collective-permute-start = (bf16[400,256]{1,0:T(8,128)(2,1)S(1)}, bf16[400,256]{1,0:T(8,128)(2,1)S(1)}, u32[]{:S(2)}, u32[]{:S(2)}) collective-permute-start(bf16[400,256]{1,0:T(8,128)(2,1)S(1)} %concatenate.10), channel_id=1, source_target_pairs={{0,2},{1,3},{2,4},{3,5},{4,6},{5,7},{6,0},{7,1},{8,10},{9,11},{10,... | collective-permute-start | bytes 614408 | tf_op jit(solution)/shard_map/ppermute | solution.py:50
  57.3 10.5 %copy-start.3 = (f32[128]{0:T(128)S(1)}, f32[128]{0:T(128)}, u32[]{:S(2)}) copy-start(f32[128]{0:T(128)} %param.12) | copy-start | bytes 1540
  57.4 9.4 %collective-permute-start.3 = (bf16[4,400,256]{2,1,0:T(8,128)(2,1)S(1)}, bf16[4,400,256]{2,1,0:T(8,128)(2,1)S(1)}, u32[]{:S(2)}, u32[]{:S(2)}) collective-permute-start(bf16[4,400,256]{2,1,0:T(8,128)(2,1)S(1)} %pad_maximum_fusion.mine_ref), channel_id=1, source_target_pairs={{0,1},{1,0},{2,3},{3,2},{4,5},{5,4},{6,7},{7,6},{8,9},{9,8},{10,11... | collective-permute-start | bytes 2457608 | tf_op jit(solution)/shard_map/ppermute | solution.py:54
  63.1 15.9 %collective-permute-start.6 = (bf16[8,32,2048]{2,1,0:T(8,128)(2,1)S(1)}, bf16[8,32,2048]{2,1,0:T(8,128)(2,1)}, u32[]{:S(2)}, u32[]{:S(2)}) collective-permute-start(bf16[8,32,2048]{2,1,0:T(8,128)(2,1)S(1)} %slice.45.refs_0_), channel_id=1, source_target_pairs={{0,56},{1,449},{2,58},{3,451},{4,60},{5,453},{6,62},{7,455},{8,0},... | collective-permute-start | bytes 3145736 | tf_op jit(solution)/shard_map/ppermute | solution.py:297
  67.8 1.1 copy-start.1
  72.6 11.1 %collective-permute-start.4 = (bf16[4,384,256]{2,1,0:T(8,128)(2,1)S(1)}, bf16[4,384,256]{2,1,0:T(8,128)(2,1)S(1)}, u32[]{:S(2)}, u32[]{:S(2)}) collective-permute-start(bf16[4,384,256]{2,1,0:T(8,128)(2,1)S(1)} %get-tuple-element.12), channel_id=1, source_target_pairs={{0,1},{1,0},{2,3},{3,2},{4,5},{5,4},{6,7},{7,6},{8,9},{9,8},{10,11... | collective-permute-start | bytes 2359304 | tf_op jit(solution)/shard_map/ppermute | solution.py:54
  74.9 17.2 %collective-permute-start.7 = (bf16[8,32,2048]{2,1,0:T(8,128)(2,1)S(1)}, bf16[8,32,2048]{2,1,0:T(8,128)(2,1)}, u32[]{:S(2)}, u32[]{:S(2)}) collective-permute-start(bf16[8,32,2048]{2,1,0:T(8,128)(2,1)S(1)} %slice.45.refs_0_), channel_id=1, source_target_pairs={{0,8},{1,65},{2,10},{3,67},{4,12},{5,69},{6,14},{7,71},{8,16},{9,7... | collective-permute-start | bytes 3145736 | tf_op jit(solution)/shard_map/ppermute | solution.py:300
  79.1 16.6 %collective-permute-start.8 = (bf16[8,32,2048]{2,1,0:T(8,128)(2,1)}, bf16[8,32,2048]{2,1,0:T(8,128)(2,1)}, u32[]{:S(2)}, u32[]{:S(2)}) collective-permute-start(bf16[8,32,2048]{2,1,0:T(8,128)(2,1)} %collective-permute-done.6.refs_1_), channel_id=1, source_target_pairs={{0,56},{1,449},{2,58},{3,451},{4,60},{5,453},{6,62},{7,455},{8,0},... | collective-permute-start | bytes 3145736 | tf_op jit(solution)/shard_map/ppermute | solution.py:297
  84.8 16.2 %all-to-all-start.2 = ((bf16[4,384,256]{2,1,0:T(8,128)(2,1)}), bf16[4,384,256]{2,1,0:T(8,128)(2,1)S(1)}, u32[]{:S(2)}, u32[]{:S(2)}) async-start(bf16[4,384,256]{2,1,0:T(8,128)(2,1)} %add_convert_fusion.1), calls=%async_computation.2 | async-start | bytes 1572864 | tf_op jit(solution)/shard_map/all_to_all | solution.py:77
  92.1 17.4 %collective-permute-start.9 = (bf16[8,32,2048]{2,1,0:T(8,128)(2,1)}, bf16[8,32,2048]{2,1,0:T(8,128)(2,1)}, u32[]{:S(2)}, u32[]{:S(2)}) collective-permute-start(bf16[8,32,2048]{2,1,0:T(8,128)(2,1)} %collective-permute-done.7.refs_2_), channel_id=1, source_target_pairs={{0,8},{1,65},{2,10},{3,67},{4,12},{5,69},{6,14},{7,71},{8,16},{9,7... | collective-permute-start | bytes 3145736 | tf_op jit(solution)/shard_map/ppermute | solution.py:300
  95.7 17.2 %collective-permute-start.10 = (bf16[8,32,2048]{2,1,0:T(8,128)(2,1)}, bf16[8,32,2048]{2,1,0:T(8,128)(2,1)}, u32[]{:S(2)}, u32[]{:S(2)}) collective-permute-start(bf16[8,32,2048]{2,1,0:T(8,128)(2,1)} %collective-permute-done.8.refs_3_), channel_id=1, source_target_pairs={{0,56},{1,449},{2,58},{3,451},{4,60},{5,453},{6,62},{7,455},{8,0},... | collective-permute-start | bytes 3145736 | tf_op jit(solution)/shard_map/ppermute | solution.py:297
  102.2 16.0 %all-to-all-start.3 = ((bf16[4,384,256]{2,1,0:T(8,128)(2,1)}), bf16[4,384,256]{2,1,0:T(8,128)(2,1)S(1)}, u32[]{:S(2)}, u32[]{:S(2)}) async-start(bf16[4,384,256]{2,1,0:T(8,128)(2,1)} %broadcast_in_dim.43), calls=%async_computation.3 | async-start | bytes 1572864 | tf_op jit(solution)/shard_map/all_to_all | solution.py:59
  109.4 19.1 %collective-permute-start.11 = (bf16[8,32,2048]{2,1,0:T(8,128)(2,1)}, bf16[8,32,2048]{2,1,0:T(8,128)(2,1)}, u32[]{:S(2)}, u32[]{:S(2)}) collective-permute-start(bf16[8,32,2048]{2,1,0:T(8,128)(2,1)} %collective-permute-done.9.refs_4_), channel_id=1, source_target_pairs={{0,8},{1,65},{2,10},{3,67},{4,12},{5,69},{6,14},{7,71},{8,16},{9,7... | collective-permute-start | bytes 3145736 | tf_op jit(solution)/shard_map/ppermute | solution.py:300
  113.0 17.2 %collective-permute-start.12 = (bf16[8,32,2048]{2,1,0:T(8,128)(2,1)}, bf16[8,32,2048]{2,1,0:T(8,128)(2,1)}, u32[]{:S(2)}, u32[]{:S(2)}) collective-permute-start(bf16[8,32,2048]{2,1,0:T(8,128)(2,1)} %collective-permute-done.10.refs_5_), channel_id=1, source_target_pairs={{0,56},{1,449},{2,58},{3,451},{4,60},{5,453},{6,62},{7,455},{8,0},... | collective-permute-start | bytes 3145736 | tf_op jit(solution)/shard_map/ppermute | solution.py:297
  118.2 7.3 %collective-permute-start.5 = (bf16[4,384,256]{2,1,0:T(8,128)(2,1)S(1)}, bf16[4,384,256]{2,1,0:T(8,128)(2,1)S(1)}, u32[]{:S(2)}, u32[]{:S(2)}) collective-permute-start(bf16[4,384,256]{2,1,0:T(8,128)(2,1)S(1)} %all-to-all-done.3.mix_ref), channel_id=1, source_target_pairs={{0,1},{1,0},{2,3},{3,2},{4,5},{5,4},{6,7},{7,6},{8,9},{9,8},{10,11... | collective-permute-start | bytes 2359304 | tf_op jit(solution)/shard_map/ppermute | solution.py:54
  125.5 1.1 copy-start.2
  137.6 7.9 %collective-permute-start.13 = (bf16[4,384,256]{2,1,0:T(8,128)(2,1)S(1)}, bf16[4,384,256]{2,1,0:T(8,128)(2,1)S(1)}, u32[]{:S(2)}, u32[]{:S(2)}) collective-permute-start(bf16[4,384,256]{2,1,0:T(8,128)(2,1)S(1)} %get-tuple-element.16), channel_id=1, source_target_pairs={{0,1},{1,0},{2,3},{3,2},{4,5},{5,4},{6,7},{7,6},{8,9},{9,8},{10,11... | collective-permute-start | bytes 2359304 | tf_op jit(solution)/shard_map/ppermute | solution.py:54
  160.0 9.0 %copy-start.6 = (f32[256]{0:T(256)S(1)}, f32[256]{0:T(256)}, u32[]{:S(2)}) copy-start(f32[256]{0:T(256)} %param.17) | copy-start | bytes 3076
  (2 other events, 2.0 us)
